TPU v7x, 32 devices: a whole 2x2x4 slice. The times are simulated.
32 devices in a mesh: sp: 8 (over z, x), tp: 4 (over y, core).
Axes of the slice: x: 2, y: 2, z: 4, core: 2. Of those that a mesh axis runs over, the one named last changes fastest.
Arguments:
- stream: bfloat16 [4096, 2048], P(('sp', 'tp')), may hold values from -6 to 6
- queries: bfloat16 [4096, 512], P('sp', 'tp'), may hold values from -6 to 6
- key_rows: bfloat16 [4096, 512], P('sp', 'tp'), may hold values from -6 to 6
- values: bfloat16 [4096, 1024], P('sp', 'tp'), may hold values from -6 to 6
- out_gate: bfloat16 [4096, 1024], P('sp', 'tp'), may hold values from -6 to 6
- fwd_decay: float32 [4096, 512], P('sp', 'tp'), may hold values from -14 to 14
- bwd_decay: float32 [4096, 512], P('sp', 'tp'), may hold values from -14 to 14
- head_gain: float32 [1024], P('tp'), may hold values from 0.1 to 1.9
- out_proj: bfloat16 [1024, 2048], replicated, may hold values from -0.1875 to 0.1875
- mix_gain: float32 [2048], replicated, may hold values from 0.1 to 1.9
- ffn_gain: float32 [2048], replicated, may hold values from 0.1 to 1.9
- moe_gain: float32 [2048], replicated, may hold values from 0.1 to 1.9
- routes: int32 [4096, 2], P(('sp', 'tp')), may hold values from 0 to 7, all different within a row; in each aligned block of 128 rows (0 to 127, 128 to 255, ...) at most 48 rows name the same one
- route_weight: float32 [4096, 2], P(('sp', 'tp')), may hold values from 0.25 to 2.5
- expert_gate: bfloat16 [8, 2048, 1024], P('sp', None, 'tp'), may hold values from -0.125 to 0.125
- expert_up: bfloat16 [8, 2048, 1024], P('sp', None, 'tp'), may hold values from -0.125 to 0.125
- expert_down: bfloat16 [8, 1024, 2048], P('sp', 'tp'), may hold values from -0.1875 to 0.1875
- shared_gate: bfloat16 [2048, 512], P(None, 'tp'), may hold values from -0.125 to 0.125
- shared_up: bfloat16 [2048, 512], P(None, 'tp'), may hold values from -0.125 to 0.125
- shared_down: bfloat16 [512, 2048], P('tp'), may hold values from -0.25 to 0.25
Outputs:
- updated: bfloat16 [4096, 2048], P(('sp', 'tp'))
Inputs may be any that keep to these rules, and one draw needn't show every extreme that they name: `routes`: each row names 2 different experts. Among the rows of one device no expert is named more than 48 times, and in every draw some device names some expert exactly 48 times.
All inputs are finite; a program needn't handle non-finite values.
Results may differ from a plain program's by a relative error of at most 0.023.
Values may be sent and summed in bfloat16 or wider, within the bound.
A program may use at most 128 MiB of HBM per device.

v0:
```python
import jax
import jax.numpy as jnp
from jax import lax
from jax.sharding import PartitionSpec as P

KEY_CHANNELS = 64
DV = 128
BLK = 64
TOPK = 2


EPS = 1e-06
GATE_NORM = 16.0
ROPE_BASE = 10000.0
TOP_PRECISION = lax.Precision.HIGHEST


def carried_in(array, axis, join, neutral, backward):
    count = lax.axis_size(axis)
    place = lax.axis_index(axis)
    ahead = count - 1 - place if backward else place
    gathered = jax.tree.map(
        lambda a, kind: lax.all_gather(a.astype(kind), axis),
        array,
        jax.tree.map(lambda a: jnp.bfloat16 if a.dtype == jnp.float32 else a.dtype, array),
    )
    state = jax.tree.map(lambda a, e: jnp.zeros_like(a) + jnp.asarray(e, a.dtype), array, neutral)

    def one(step, state):
        source = count - 1 - step if backward else step
        return join(
            state,
            jax.tree.map(
                lambda a, own: lax.dynamic_index_in_dim(a, source, 0, False).astype(own.dtype),
                gathered,
                array,
            ),
        )

    return lax.fori_loop(0, ahead, one, state)


def normalize(tensor):
    return tensor * lax.rsqrt(jnp.mean(tensor * tensor, axis=-1, keepdims=True) + EPS)


def rotate(tensor, positions):
    half_width = tensor.shape[-1] // 2
    frequency = ROPE_BASE ** (-jnp.arange(half_width, dtype=jnp.float32) / half_width)
    angles = positions[:, None] * frequency[None, :]
    cosine = jnp.cos(angles)[:, None, :]
    sine_part = jnp.sin(angles)[:, None, :]
    front_half = tensor[..., :half_width]
    back_half = tensor[..., half_width:]
    return jnp.concatenate(
        [front_half * cosine - back_half * sine_part, front_half * sine_part + back_half * cosine],
        axis=-1,
    )


def blockwise(query_rows, key_data, value_matrix, log_decay, start_state):
    length, head_count, key_width = query_rows.shape
    value_width = value_matrix.shape[-1]
    block_count = length // BLK
    query_blocks = query_rows.reshape(block_count, BLK, head_count, key_width)
    key_blocks = key_data.reshape(block_count, BLK, head_count, key_width)
    value_blocks = value_matrix.reshape(block_count, BLK, head_count, value_width)
    cumul = jnp.cumsum(log_decay.reshape(block_count, BLK, head_count, key_width), axis=1)
    middle = cumul[:, BLK // 2 - 1 : BLK // 2]
    query_scaled = query_blocks * jnp.exp(cumul - middle)
    key_scaled = key_blocks * jnp.exp(middle - cumul)
    scores = jnp.einsum("nthk,nshk->nhts", query_scaled, key_scaled, precision=TOP_PRECISION)
    lower_mask = jnp.arange(BLK)[:, None] >= jnp.arange(BLK)[None, :]
    scores = jnp.where(lower_mask, scores, 0.0)
    within = jnp.einsum("nhts,nshv->nthv", scores, value_blocks, precision=TOP_PRECISION)
    last_cumul = cumul[:, -1:]
    query_in = query_blocks * jnp.exp(cumul)
    key_out = key_blocks * jnp.exp(last_cumul - cumul)
    block_decay = jnp.exp(last_cumul[:, 0])

    def advance(carried_state, pieces):
        query_segment, key_segment, value_segment, decay_segment = pieces
        across_blocks = jnp.einsum(
            "asu,sun->asn", query_segment, carried_state, precision=TOP_PRECISION
        )
        carried_state = carried_state * decay_segment[:, :, None] + jnp.einsum(
            "jco,jcm->com", key_segment, value_segment, precision=TOP_PRECISION
        )
        return (carried_state, across_blocks)

    final_state, across_blocks = lax.scan(
        advance, start_state, (query_in, key_out, value_blocks, block_decay)
    )
    return ((within + across_blocks).reshape(length, head_count, value_width), final_state)


def summarize(key_data, value_matrix, log_decay):
    cumul = jnp.cumsum(log_decay, axis=0)
    grand_total = cumul[-1]
    weighted_rows = key_data * jnp.exp(grand_total[None] - cumul)
    return (
        jnp.exp(grand_total),
        jnp.einsum("jco,jcm->com", weighted_rows, value_matrix, precision=TOP_PRECISION),
    )


def compose(earlier, later):
    return (earlier[0] * later[0], earlier[1] * later[0][:, :, None] + later[1])


def feed_forward(row_data, gate_mat, up_mat, down_mat):
    hidden = (
        jax.nn.silu(jnp.dot(row_data, gate_mat, preferred_element_type=jnp.float32))
        * jnp.dot(row_data, up_mat, preferred_element_type=jnp.float32)
    ).astype(jnp.bfloat16)
    return jnp.dot(hidden, down_mat, preferred_element_type=jnp.float32)


def place_slots(route_block, experts):
    flat_ids = route_block.reshape(-1)
    onehot = (flat_ids[:, None] == jnp.arange(experts, dtype=jnp.int32)[None, :]).astype(jnp.int32)
    before = jnp.cumsum(onehot, axis=0) - onehot
    return (flat_ids, jnp.sum(before * onehot, axis=1))


def fill_slots(row_data, route_block, experts, capacity):
    flat_ids, slot_ids = place_slots(route_block, experts)
    token_ids = jnp.arange(flat_ids.shape[0], dtype=jnp.int32) // route_block.shape[1]
    buffer = jnp.zeros((experts, capacity, row_data.shape[1]), row_data.dtype)
    return buffer.at[flat_ids, slot_ids].set(row_data[token_ids])


def body(
    stream,
    queries,
    key_rows,
    values,
    out_gate,
    fwd_decay,
    bwd_decay,
    head_gain,
    out_proj,
    mix_gain,
    ffn_gain,
    moe_gain,
    routes,
    route_weight,
    expert_gate,
    expert_up,
    expert_down,
    shared_gate,
    shared_up,
    shared_down,
):
    tokens_here = stream.shape[0]
    span_rows = queries.shape[0]
    heads_here = queries.shape[1] // KEY_CHANNELS
    offset = lax.axis_index("sp") * span_rows
    positions = (offset + jnp.arange(span_rows, dtype=jnp.int32)).astype(jnp.float32)
    query_rows = rotate(
        queries.astype(jnp.float32).reshape(span_rows, heads_here, KEY_CHANNELS)
        * KEY_CHANNELS ** (-0.5),
        positions,
    )
    key_data = rotate(
        key_rows.astype(jnp.float32).reshape(span_rows, heads_here, KEY_CHANNELS), positions
    )
    value_matrix = values.astype(jnp.float32).reshape(span_rows, heads_here, DV)
    fwd_log = jax.nn.log_sigmoid(fwd_decay).reshape(span_rows, heads_here, KEY_CHANNELS) / GATE_NORM
    bwd_log = (
        jax.nn.log_sigmoid(bwd_decay[::-1]).reshape(span_rows, heads_here, KEY_CHANNELS) / GATE_NORM
    )
    query_back = query_rows[::-1]
    key_back = key_data[::-1]
    value_back = value_matrix[::-1]
    zero_state = jnp.zeros((heads_here, KEY_CHANNELS, DV), jnp.float32)
    identity = (jnp.ones((heads_here, KEY_CHANNELS), jnp.float32), zero_state)
    fwd_summary = summarize(key_data, value_matrix, fwd_log)
    bwd_summary = summarize(key_back, value_back, bwd_log)
    fwd_carry = carried_in(fwd_summary, "sp", compose, identity, False)[1]
    bwd_carry = carried_in(bwd_summary, "sp", compose, identity, True)[1]
    fwd_out, _ = blockwise(query_rows, key_data, value_matrix, fwd_log, fwd_carry)
    bwd_out, _ = blockwise(query_back, key_back, value_back, bwd_log, bwd_carry)
    combined = normalize(fwd_out + bwd_out[::-1]) * head_gain.reshape(heads_here, DV)
    head_mixed = (
        combined.reshape(span_rows, -1) * jax.nn.silu(out_gate.astype(jnp.float32))
    ).astype(jnp.bfloat16)
    mixed_out = lax.all_to_all(head_mixed, "tp", split_axis=0, concat_axis=1, tiled=True)
    projected = jnp.dot(mixed_out, out_proj, preferred_element_type=jnp.float32)
    residual = (stream.astype(jnp.float32) + normalize(projected) * mix_gain).astype(jnp.bfloat16)
    normed = (normalize(residual.astype(jnp.float32)) * ffn_gain).astype(jnp.bfloat16)
    experts = lax.axis_size("sp")
    groups = lax.axis_size("tp")
    capacity = max(2, 3 * tokens_here * TOPK // (2 * experts))
    model_width = normed.shape[1]
    arrived = lax.all_to_all(
        fill_slots(normed, routes, experts, capacity), "sp", split_axis=0, concat_axis=0, tiled=True
    )
    fanned, shared_flat = (
        lax.all_gather(arrived.reshape(experts * capacity, model_width), "tp", axis=0, tiled=True),
        lax.all_gather(normed, "tp", axis=0, tiled=True),
    )
    routed_rows = fanned.reshape(groups, experts * capacity, model_width)
    shared_rows = shared_flat.reshape(groups, tokens_here, model_width)
    width_rows = experts * capacity + tokens_here
    number = width_rows * lax.axis_size("tp") // width_rows
    routed_part = routed_rows.reshape(number * experts * capacity, model_width)
    shared_part = shared_rows.reshape(number * tokens_here, model_width)
    routed_out = feed_forward(routed_part, expert_gate[0], expert_up[0], expert_down[0]).reshape(
        number, experts * capacity, model_width
    )
    shared_out = feed_forward(shared_part, shared_gate, shared_up, shared_down).reshape(
        number, tokens_here, model_width
    )
    summed = lax.psum_scatter(
        jnp.concatenate([routed_out, shared_out], axis=1)
        .reshape(width_rows * lax.axis_size("tp"), model_width)
        .astype(jnp.bfloat16),
        "tp",
        scatter_dimension=0,
        tiled=True,
    ).astype(jnp.float32)
    routed_done = (
        summed[: experts * capacity].astype(jnp.bfloat16).reshape(experts, capacity, model_width)
    )
    routed_back = lax.all_to_all(routed_done, "sp", split_axis=0, concat_axis=0, tiled=True)
    shared_sum = summed[experts * capacity :]
    flat_ids, slot_ids = place_slots(routes, experts)
    picked = routed_back.reshape(experts * capacity, model_width)[flat_ids * capacity + slot_ids]
    picked = picked.astype(jnp.float32).reshape(tokens_here, TOPK, model_width)
    mixture = shared_sum + jnp.sum(picked * route_weight[:, :, None], axis=1)
    return (residual.astype(jnp.float32) + normalize(mixture) * moe_gain).astype(jnp.bfloat16)


def solution(mesh):
    return jax.shard_map(
        body,
        mesh=mesh,
        in_specs=(
            P(("sp", "tp"), None),
            P("sp", "tp"),
            P("sp", "tp"),
            P("sp", "tp"),
            P("sp", "tp"),
            P("sp", "tp"),
            P("sp", "tp"),
            P("tp"),
            P(),
            P(),
            P(),
            P(),
            P(("sp", "tp"), None),
            P(("sp", "tp"), None),
            P("sp", None, "tp"),
            P("sp", None, "tp"),
            P("sp", "tp", None),
            P(None, "tp"),
            P(None, "tp"),
            P("tp", None),
        ),
        out_specs=P(("sp", "tp"), None),
        check_vma=False,
    )
```

profile of v0, /device:TPU:0, one launch (start us, length us, event | category | flops | bytes accessed | tf_op | source)
XLA Modules:
  0.0 532.0 jit_solution(1066690131067379071)
XLA Ops:
  8.8 13.0 %fusion.54 = f32[8,64,2,64]{3,0,1,2:T(8,128)S(1)} fusion(f32[8,64,2,64]{3,0,1,2:T(8,128)S(1)} %copy.187), kind=kOutput, calls=%fused_computation.152 | output fusion | flops 4128768 | bytes 524288 | tf_op jit(solution)/shard_map/jit(cumsum)/reduce_window_sum | solution.py:68
  26.9 2.0 copy.215
  37.4 2.4 reduce-window.20
  41.0 1.2 copy.250
  43.2 3.5 multiply_subtract_fusion.1
  46.6 1.8 exponential_multiply_fusion.7
  49.1 32.6 %all-gather = bf16[16,64,128]{2,1,0:T(8,128)(2,1)S(1)} all-gather(bf16[2,64,128]{2,1,0:T(8,128)(2,1)S(1)} %convolution_convert_fusion.3), channel_id=2, replica_groups=mesh['sp'=8,'tp'=4] {'sp'}, dimensions={0}, use_global_device_ids=true | all-gather | bytes 294912 | tf_op jit(solution)/shard_map/all_gather | solution.py:23
  81.6 20.5 %all_gather.26 = bf16[8,2,64]{2,1,0:T(2,128)(2,1)S(1)} all-gather(bf16[1,2,64]{2,1,0:T(2,128)(2,1)S(1)} %get-tuple-element.375), channel_id=1, replica_groups=mesh['sp'=8,'tp'=4] {'sp'}, dimensions={0}, use_global_device_ids=true | all-gather | bytes 2304 | tf_op jit(solution)/shard_map/all_gather | solution.py:23
  102.3 1.2 copy.210
  104.5 1.8 pad_maximum_fusion.1
  107.3 1.9 exponential_multiply_fusion.9
  110.0 31.8 %while.51 = (s32[]{:T(128)}, f32[2,64,128]{2,1,0:T(8,128)S(1)}, f32[8,64,2,128]{3,1,2,0:T(8,128)}, f32[8,2,64]{2,0,1:T(8,128)}, f32[8,64,2,64]{3,0,1,2:T(8,128)}...) while((s32[]{:T(128)}, f32[2,64,128]{2,1,0:T(8,128)S(1)}, ...), condition=%wide.region_6.7_spmd, body=%wide.region_5.6_spmd.sunk | while | flops 25198592 | bytes 526941 | solution.py:91
  110.0 1.3 constant_dynamic-slice_fusion.10
  114.1 1.3 constant_dynamic-slice_fusion.10
  118.0 1.3 constant_dynamic-slice_fusion.10
  122.0 1.3 constant_dynamic-slice_fusion.10
  126.0 1.3 constant_dynamic-slice_fusion.10
  130.0 1.3 constant_dynamic-slice_fusion.10
  133.9 1.3 constant_dynamic-slice_fusion.10
  137.9 1.3 constant_dynamic-slice_fusion.10
  143.0 1.4 fusion.10
  144.5 2.4 reduce-window.24
  147.7 1.2 exponential_multiply_fusion.2
  149.9 2.1 convolution_convert_fusion.2
  151.9 30.7 %all-gather.1 = bf16[16,64,128]{2,1,0:T(8,128)(2,1)S(1)} all-gather(bf16[2,64,128]{2,1,0:T(8,128)(2,1)S(1)} %convolution_convert_fusion.2), channel_id=3, replica_groups=mesh['sp'=8,'tp'=4] {'sp'}, dimensions={0}, use_global_device_ids=true | all-gather | bytes 294912 | tf_op jit(solution)/shard_map/all_gather | solution.py:23
  182.7 17.0 %all_gather.29 = bf16[8,2,64]{2,1,0:T(2,128)(2,1)S(1)} all-gather(bf16[1,2,64]{2,1,0:T(2,128)(2,1)S(1)} %get-tuple-element.382), channel_id=1, replica_groups=mesh['sp'=8,'tp'=4] {'sp'}, dimensions={0}, use_global_device_ids=true | all-gather | bytes 2304 | tf_op jit(solution)/shard_map/all_gather | solution.py:23
  201.5 3.1 exponential_multiply_fusion.4
  205.4 31.9 %while.53 = (s32[]{:T(128)}, f32[2,64,128]{2,1,0:T(8,128)S(1)}, f32[8,64,2,128]{3,1,2,0:T(8,128)}, f32[8,2,64]{2,0,1:T(8,128)}, f32[8,64,2,64]{3,0,1,2:T(8,128)}...) while((s32[]{:T(128)}, f32[2,64,128]{2,1,0:T(8,128)S(1)}, ...), condition=%wide.region_13.14_spmd, body=%wide.region_12.13_spmd.sunk | while | flops 25198592 | bytes 526941 | solution.py:91
  205.4 1.3 constant_dynamic-slice_fusion.12
  208.3 1.1 convolution_add_fusion.5
  209.4 1.3 constant_dynamic-slice_fusion.12
  212.2 1.1 convolution_add_fusion.5
  213.4 1.3 constant_dynamic-slice_fusion.12
  216.2 1.1 convolution_add_fusion.5
  217.4 1.3 constant_dynamic-slice_fusion.12
  220.2 1.1 convolution_add_fusion.5
  221.4 1.3 constant_dynamic-slice_fusion.12
  224.2 1.1 convolution_add_fusion.5
  225.4 1.3 constant_dynamic-slice_fusion.12
  228.2 1.1 convolution_add_fusion.5
  229.4 1.3 constant_dynamic-slice_fusion.12
  233.3 1.3 constant_dynamic-slice_fusion.12
  236.2 1.1 convolution_add_fusion.5
  238.4 1.7 fusion.9
  242.6 3.4 all-to-all-start
  247.3 4.6 all-to-all-done
  252.1 3.1 multiply_reduce_fusion.2
  258.5 2.3 gather_fusion
  261.0 33.4 %scatter_fusion = bf16[8,48,2048]{2,1,0:T(8,128)(2,1)S(1)} fusion(bf16[8,48,2048]{2,1,0:T(8,128)(2,1)S(1)} %broadcast_in_dim.32, s32[256]{0:T(256)S(1)} %bitcast.224, bf16[256,2048]{1,0:T(8,128)(2,1)} %gather_fusion), kind=kCustom, calls=%fused_computation.2 | custom fusion | bytes 3147776 | tf_op jit(solution)/shard_map/scatter | solution.py:130
  294.3 40.1 %all_to_all.29 = bf16[8,48,2048]{2,1,0:T(8,128)(2,1)} all-to-all(bf16[8,48,2048]{2,1,0:T(8,128)(2,1)S(1)} %scatter_fusion), channel_id=1, replica_groups=mesh['sp'=8,'tp'=4] {'sp'}, dimensions={0} | all-to-all | bytes 3145728 | tf_op jit(solution)/shard_map/all_to_all | solution.py:196
  334.6 2.5 fusion.56
  337.1 4.9 convolution_convert_fusion.1
  342.0 37.3 %all-gather.5.cloned.1.call-done = bf16[1536,2048]{1,0:T(8,128)(2,1)} async-done(((bf16[384,2048]{1,0:T(8,128)(2,1)}), bf16[1536,2048]{1,0:T(8,128)(2,1)}) %all-gather.5.cloned.1.call-update) | async-done | bytes 6291472 | tf_op jit(solution)/shard_map/all_gather | solution.py:200
  379.3 5.1 fusion.18
  384.4 2.1 fusion.8
  386.5 4.5 convolution_convert_fusion
  391.0 7.6 %pad_maximum_fusion = bf16[4,512,2048]{2,1,0:T(8,128)(2,1)} fusion(bf16[4,128,2048]{2,1,0:T(8,128)(2,1)S(1)} %bitcast.226, bf16[4,384,2048]{2,1,0:T(8,128)(2,1)} %convolution_convert_fusion), kind=kLoop, calls=%fused_computation.25 | loop fusion | flops 16777216 | bytes 16777216 | tf_op jit(solution)/shard_map/concatenate | solution.py:216
  398.7 71.5 %reduce-scatter.2.cloned.1.call-done = bf16[512,2048]{1,0:T(8,128)(2,1)} async-done(((bf16[2048,2048]{1,0:T(8,128)(2,1)}), bf16[512,2048]{1,0:T(8,128)(2,1)}) %reduce-scatter.2.cloned.1.call-update) | async-done | bytes 2097168 | tf_op jit(solution)/shard_map/reduce_scatter | solution.py:215
  470.2 2.8 slice.99
  473.0 5.9 %all-to-all-start.2 = ((bf16[8,48,2048]{2,1,0:T(8,128)(2,1)}), bf16[8,48,2048]{2,1,0:T(8,128)(2,1)S(1)}, u32[]{:S(2)}, u32[]{:S(2)}) async-start(bf16[8,48,2048]{2,1,0:T(8,128)(2,1)} %bitcast.232), calls=%async_computation.3 | async-start | bytes 3145728 | tf_op jit(solution)/shard_map/all_to_all | solution.py:226
  479.1 36.7 %all-to-all-done.2 = bf16[8,48,2048]{2,1,0:T(8,128)(2,1)S(1)} async-done(((bf16[8,48,2048]{2,1,0:T(8,128)(2,1)}), bf16[8,48,2048]{2,1,0:T(8,128)(2,1)S(1)}, u32[]{:S(2)}, u32[]{:S(2)}) %all-to-all-start.2) | async-done | bytes 1572896 | tf_op jit(solution)/shard_map/all_to_all | solution.py:226
  515.7 2.3 gather_fusion.1
  518.1 2.4 reshape.375
  520.5 3.2 multiply_reduce_fusion
  (229 shorter events, 72.0 us)
Async XLA Ops:
  6.5 379.9 %copy-start = (bf16[1,256,2048]{2,1,0:T(8,128)(2,1)S(1)}, bf16[1,256,2048]{2,1,0:T(8,128)(2,1)}, u32[]{:S(2)}) copy-start(bf16[1,256,2048]{2,1,0:T(8,128)(2,1)} %param.44) | copy-start | bytes 3145732
  6.5 16.7 %copy-start.7 = (bf16[512,256]{1,0:T(8,128)(2,1)S(1)}, bf16[512,256]{1,0:T(8,128)(2,1)}, u32[]{:S(2)}) copy-start(bf16[512,256]{1,0:T(8,128)(2,1)} %param.31) | copy-start | bytes 786436
  8.8 16.5 %copy-start.20 = (f32[512,128]{1,0:T(8,128)S(1)}, f32[512,128]{1,0:T(8,128)}, u32[]{:S(2)}) copy-start(f32[512,128]{1,0:T(8,128)} %param.34) | copy-start | bytes 786436
  21.8 0.8 copy-start.10
  25.4 6.7 %copy-start.22 = (bf16[512,128]{1,0:T(8,128)(2,1)S(1)}, bf16[512,128]{1,0:T(8,128)(2,1)}, u32[]{:S(2)}) copy-start(bf16[512,128]{1,0:T(8,128)(2,1)} %param.29) | copy-start | bytes 393220
  30.1 0.8 copy-start.8
  35.3 6.9 %copy-start.29 = (f32[512]{0:T(512)S(1)}, f32[512]{0:T(512)}, u32[]{:S(2)}) copy-start(f32[512]{0:T(512)} %add_convert_fusion.1) | copy-start | bytes 6148
  35.3 6.9 %copy-start.33 = (f32[32]{0:T(128)S(1)}, f32[32]{0:T(128)}, u32[]{:S(2)}) copy-start(f32[32]{0:T(128)} %multiply_power_fusion) | copy-start | bytes 388
  42.2 4.5 copy-start.12
  103.5 3.8 copy-start.11
  103.5 3.8 copy-start.24
  103.5 3.8 copy-start.25
  109.2 32.7 %copy-start.15 = (f32[8,64,2,64]{3,0,1,2:T(8,128)S(1)}, f32[8,64,2,64]{3,0,1,2:T(8,128)}, u32[]{:S(2)}) copy-start(f32[8,64,2,64]{3,0,1,2:T(8,128)} %get-tuple-element.361) | copy-start | bytes 786436
  109.2 32.7 %copy-start.16 = (f32[8,64,2,64]{3,0,1,2:T(8,128)S(1)}, f32[8,64,2,64]{3,0,1,2:T(8,128)}, u32[]{:S(2)}) copy-start(f32[8,64,2,64]{3,0,1,2:T(8,128)} %get-tuple-element.370) | copy-start | bytes 786436
  110.0 32.9 %copy-start.18 = (bf16[8,64,2,128]{3,2,1,0:T(2,128)(2,1)S(1)}, bf16[8,64,2,128]{3,2,1,0:T(2,128)(2,1)}, u32[]{:S(2)}) copy-start(bf16[8,64,2,128]{3,2,1,0:T(2,128)(2,1)} %reshape_reshape.5) | copy-start | bytes 786436
  144.5 4.4 copy-start.17
  149.6 51.8 %copy-start.9 = (f32[8,64,2,64]{3,0,1,2:T(8,128)S(1)}, f32[8,64,2,64]{3,0,1,2:T(8,128)}, u32[]{:S(2)}) copy-start(f32[8,64,2,64]{3,0,1,2:T(8,128)} %copy-done.8) | copy-start | bytes 786436
  149.7 51.8 %copy-start.23 = (f32[8,2,64]{2,0,1:T(8,128)S(1)}, f32[8,2,64]{2,0,1:T(8,128)}, u32[]{:S(2)}) copy-start(f32[8,2,64]{2,0,1:T(8,128)} %get-tuple-element.378) | copy-start | bytes 12292
  204.6 32.8 %copy-start.13 = (f32[8,64,2,64]{3,0,1,2:T(8,128)S(1)}, f32[8,64,2,64]{3,0,1,2:T(8,128)}, u32[]{:S(2)}) copy-start(f32[8,64,2,64]{3,0,1,2:T(8,128)} %get-tuple-element.365) | copy-start | bytes 786436
  204.6 32.8 %copy-start.14 = (f32[8,64,2,64]{3,0,1,2:T(8,128)S(1)}, f32[8,64,2,64]{3,0,1,2:T(8,128)}, u32[]{:S(2)}) copy-start(f32[8,64,2,64]{3,0,1,2:T(8,128)} %get-tuple-element.372) | copy-start | bytes 786436
  240.1 0.7 copy-start.32
  240.4 1.0 copy-start.21
  241.0 5.2 copy-start.30
  242.6 9.4 %all-to-all-start = ((bf16[4,128,256]{2,1,0:T(8,128)(2,1)}), bf16[4,128,256]{2,1,0:T(8,128)(2,1)S(1)}, u32[]{:S(2)}, u32[]{:S(2)}) async-start(bf16[4,128,256]{2,1,0:T(8,128)(2,1)} %bitcast.51), calls=%async_computation | async-start | bytes 524288 | tf_op jit(solution)/shard_map/all_to_all | solution.py:188
  246.0 88.6 %all-gather.7.cloned.1.call-start = ((), (), s32[]{:S(2)}) async-start(), calls=%async_computation.5 | async-start | bytes 2621440 | tf_op jit(solution)/shard_map/all_gather | solution.py:201
  252.1 3.1 copy-start.19
  252.1 3.1 copy-start.26
  255.2 1.2 copy-start.27
  255.6 0.8 copy-start.4
  257.4 1.0 copy-start.1
  257.4 121.9 %all-gather.5.cloned.1.call-start = ((), (), s32[]{:S(2)}) async-start(), calls=%async_computation.4 | async-start | bytes 7864320 | tf_op jit(solution)/shard_map/all_gather | solution.py:200
  334.5 135.7 %reduce-scatter.2.cloned.1.call-start = ((), (), s32[]{:S(2)}) async-start(), calls=%async_computation.6 | async-start | bytes 10485760 | tf_op jit(solution)/shard_map/reduce_scatter | solution.py:215
  334.6 2.6 copy-start.2
  342.0 42.4 %copy-start.35 = (bf16[1,2048,256]{2,1,0:T(8,128)(2,1)S(1)}, bf16[1,2048,256]{2,1,0:T(8,128)(2,1)}, u32[]{:S(2)}) copy-start(bf16[1,2048,256]{2,1,0:T(8,128)(2,1)} %param.43) | copy-start | bytes 3145732
  379.3 5.1 copy-start.34
  386.5 4.5 copy-start.3
  473.0 5.9 %copy-start.31 = (f32[128,2]{0,1:T(2,128)S(1)}, f32[128,2]{0,1:T(2,128)}, u32[]{:S(2)}) copy-start(f32[128,2]{0,1:T(2,128)} %param.41) | copy-start | bytes 3076
  473.0 42.7 %all-to-all-start.2 = ((bf16[8,48,2048]{2,1,0:T(8,128)(2,1)}), bf16[8,48,2048]{2,1,0:T(8,128)(2,1)S(1)}, u32[]{:S(2)}, u32[]{:S(2)}) async-start(bf16[8,48,2048]{2,1,0:T(8,128)(2,1)} %bitcast.232), calls=%async_computation.3 | async-start | bytes 3145728 | tf_op jit(solution)/shard_map/all_to_all | solution.py:226
  520.4 3.2 copy-start.6
  520.4 3.5 copy-start.5
  520.5 3.5 copy-start.28
Sparse Core Ops, SparseCore 0:
  257.6 19.4 all-gather.6
  334.6 44.6 all-gather.4
  398.8 71.3 reduce-scatter.1
where the time goes:
time: 541 us; the launch traced here: 532 us
  waiting for transfers between devices  150 us (28%)
  blocking collectives  141 us (26%)
  local copies, waits for them, and re-layouts  102 us (19%)
  matrix products  61.4 us (11%)
  other arithmetic  52.3 us (10%)
  between operations  14.3 us (3%)
  starting transfers between devices  9.67 us (2%)
    all_gather x4, blocking collectives, carried_in(): lax.all_gather(a.astype(kind), axis)  101 us
    reduce_scatter x1, waiting for transfers between devices, body(): lax.psum_scatter(jnp.concatenate([routed_out, shared_out], axis=1).reshap...  71.5 us
    all_to_all x1, blocking collectives, body(): lax.all_to_all(fill_slots(normed, routes, experts, capacity), 'sp', split...  40.1 us
    all_gather x1, waiting for transfers between devices, body(): lax.all_gather(arrived.reshape(experts * capacity, model_width), 'tp', ax...  37.3 us
    all_to_all x1, waiting for transfers between devices, body(): lax.all_to_all(routed_done, 'sp', split_axis=0, concat_axis=0, tiled=True)  36.7 us
    scatter x1, local copies, waits for them, and re-layouts, fill_slots(): return buffer.at[flat_ids, slot_ids].set(row_data[token_ids])  33.4 us
    dynamic_slice x32, local copies, waits for them, and re-layouts, blockwise(): lax.scan(advance, start_state, (query_in, key_out, value_blocks, block_de...  32 us
    dot_general x16, matrix products, advance(): jnp.einsum('jco,jcm->com', key_segment, value_segment, precision=TOP_PREC...  18.1 us
  transfers between devices with their start and end apart: 5, of which 4 were waited for; matrix products, arithmetic and copies ran while one was open for 8% of the time, Pallas kernels for 0%

commit v1 on v0

v1 whole, which is shorter than its diff:
```python
import jax
import jax.numpy as jnp
from jax import lax
from jax.sharding import PartitionSpec as P

KEY_CHANNELS = 64
DV = 128
BLK = 64
TOPK = 2


EPS = 1e-06
GATE_NORM = 16.0
ROPE_BASE = 10000.0
TOP_PRECISION = lax.Precision.HIGHEST


def carried_in(fwd_summary, bwd_summary, axis):
    count = lax.axis_size(axis)
    place = lax.axis_index(axis)
    decays = jnp.stack([fwd_summary[0], bwd_summary[0]])
    states = jnp.stack([fwd_summary[1], bwd_summary[1]])
    width = states.shape[-1]
    packed = jnp.concatenate(
        [states.reshape(-1, width), decays.reshape(-1, width)], axis=0
    ).astype(jnp.bfloat16)
    gathered = lax.all_gather(packed, axis).astype(jnp.float32)
    state_rows = states.size // width
    all_states = gathered[:, :state_rows].reshape((count,) + states.shape)
    all_decays = gathered[:, state_rows:].reshape((count,) + decays.shape)
    fwd = jnp.zeros_like(states[0])
    bwd = jnp.zeros_like(states[0])
    for step in range(count):
        fwd = jnp.where(
            step < place, fwd * all_decays[step, 0][:, :, None] + all_states[step, 0], fwd
        )
        source = count - 1 - step
        bwd = jnp.where(
            source > place, bwd * all_decays[source, 1][:, :, None] + all_states[source, 1], bwd
        )
    return fwd, bwd


def normalize(tensor):
    return tensor * lax.rsqrt(jnp.mean(tensor * tensor, axis=-1, keepdims=True) + EPS)


def rotate(tensor, positions):
    half_width = tensor.shape[-1] // 2
    frequency = ROPE_BASE ** (-jnp.arange(half_width, dtype=jnp.float32) / half_width)
    angles = positions[:, None] * frequency[None, :]
    cosine = jnp.cos(angles)[:, None, :]
    sine_part = jnp.sin(angles)[:, None, :]
    front_half = tensor[..., :half_width]
    back_half = tensor[..., half_width:]
    return jnp.concatenate(
        [front_half * cosine - back_half * sine_part, front_half * sine_part + back_half * cosine],
        axis=-1,
    )


def blockwise(query_rows, key_data, value_matrix, log_decay, start_state):
    length, head_count, key_width = query_rows.shape
    value_width = value_matrix.shape[-1]
    block_count = length // BLK
    query_blocks = query_rows.reshape(block_count, BLK, head_count, key_width)
    key_blocks = key_data.reshape(block_count, BLK, head_count, key_width)
    value_blocks = value_matrix.reshape(block_count, BLK, head_count, value_width)
    cumul = jnp.cumsum(log_decay.reshape(block_count, BLK, head_count, key_width), axis=1)
    middle = cumul[:, BLK // 2 - 1 : BLK // 2]
    query_scaled = query_blocks * jnp.exp(cumul - middle)
    key_scaled = key_blocks * jnp.exp(middle - cumul)
    scores = jnp.einsum("nthk,nshk->nhts", query_scaled, key_scaled, precision=TOP_PRECISION)
    lower_mask = jnp.arange(BLK)[:, None] >= jnp.arange(BLK)[None, :]
    scores = jnp.where(lower_mask, scores, 0.0)
    within = jnp.einsum("nhts,nshv->nthv", scores, value_blocks, precision=TOP_PRECISION)
    last_cumul = cumul[:, -1:]
    query_in = query_blocks * jnp.exp(cumul)
    key_out = key_blocks * jnp.exp(last_cumul - cumul)
    block_decay = jnp.exp(last_cumul[:, 0])

    def advance(carried_state, pieces):
        query_segment, key_segment, value_segment, decay_segment = pieces
        across_blocks = jnp.einsum(
            "asu,sun->asn", query_segment, carried_state, precision=TOP_PRECISION
        )
        carried_state = carried_state * decay_segment[:, :, None] + jnp.einsum(
            "jco,jcm->com", key_segment, value_segment, precision=TOP_PRECISION
        )
        return (carried_state, across_blocks)

    final_state, across_blocks = lax.scan(
        advance,
        start_state,
        (query_in, key_out, value_blocks, block_decay),
        unroll=block_count,
    )
    return ((within + across_blocks).reshape(length, head_count, value_width), final_state)


def summarize(key_data, value_matrix, log_decay):
    cumul = jnp.cumsum(log_decay, axis=0)
    grand_total = cumul[-1]
    weighted_rows = key_data * jnp.exp(grand_total[None] - cumul)
    return (
        jnp.exp(grand_total),
        jnp.einsum("jco,jcm->com", weighted_rows, value_matrix, precision=TOP_PRECISION),
    )


def feed_forward(row_data, gate_parts, up_parts, down_mat):
    groups, _, width = gate_parts.shape
    total = jnp.zeros((row_data.shape[0], down_mat.shape[1]), jnp.float32)
    for group in range(groups):
        hidden = (
            jax.nn.silu(jnp.dot(row_data, gate_parts[group], preferred_element_type=jnp.float32))
            * jnp.dot(row_data, up_parts[group], preferred_element_type=jnp.float32)
        ).astype(jnp.bfloat16)
        total = total + jnp.dot(
            hidden,
            down_mat[group * width : (group + 1) * width],
            preferred_element_type=jnp.float32,
        )
    return total


def slot_map(route_block, experts, capacity):
    tokens, choices = route_block.shape
    flat_ids = route_block.reshape(-1)
    total = flat_ids.shape[0]
    onehot = (flat_ids[:, None] == jnp.arange(experts, dtype=jnp.int32)[None, :]).astype(
        jnp.bfloat16
    )
    earlier = (jnp.arange(total)[:, None] > jnp.arange(total)[None, :]).astype(jnp.bfloat16)
    before = jnp.dot(earlier, onehot, preferred_element_type=jnp.float32)
    slot_ids = jnp.sum(before * onehot.astype(jnp.float32), axis=1).astype(jnp.int32)
    return (flat_ids * capacity + slot_ids).reshape(tokens, choices)


def body(
    stream,
    queries,
    key_rows,
    values,
    out_gate,
    fwd_decay,
    bwd_decay,
    head_gain,
    out_proj,
    mix_gain,
    ffn_gain,
    moe_gain,
    routes,
    route_weight,
    expert_gate,
    expert_up,
    expert_down,
    shared_gate,
    shared_up,
    shared_down,
):
    tokens_here = stream.shape[0]
    span_rows = queries.shape[0]
    heads_here = queries.shape[1] // KEY_CHANNELS
    experts = lax.axis_size("sp")
    capacity = max(2, 3 * tokens_here * TOPK // (2 * experts))
    gate_parts = lax.all_gather(expert_gate[0], "tp")
    up_parts = lax.all_gather(expert_up[0], "tp")
    down_mat = lax.all_gather(expert_down[0], "tp", axis=0, tiled=True)
    shared_gate_parts = lax.all_gather(shared_gate, "tp")
    shared_up_parts = lax.all_gather(shared_up, "tp")
    shared_down_mat = lax.all_gather(shared_down, "tp", axis=0, tiled=True)
    rows_of = slot_map(routes, experts, capacity)
    slots = jnp.arange(experts * capacity, dtype=jnp.int32)
    taken = rows_of[:, :, None] == slots[None, None, :]
    pick = jnp.any(taken, axis=1).astype(jnp.bfloat16)
    weights = jnp.sum(jnp.where(taken, route_weight[:, :, None], 0.0), axis=1)
    weights_high = weights.astype(jnp.bfloat16)
    weights_low = (weights - weights_high.astype(jnp.float32)).astype(jnp.bfloat16)
    offset = lax.axis_index("sp") * span_rows
    positions = (offset + jnp.arange(span_rows, dtype=jnp.int32)).astype(jnp.float32)
    query_rows = rotate(
        queries.astype(jnp.float32).reshape(span_rows, heads_here, KEY_CHANNELS)
        * KEY_CHANNELS ** (-0.5),
        positions,
    )
    key_data = rotate(
        key_rows.astype(jnp.float32).reshape(span_rows, heads_here, KEY_CHANNELS), positions
    )
    value_matrix = values.astype(jnp.float32).reshape(span_rows, heads_here, DV)
    fwd_log = jax.nn.log_sigmoid(fwd_decay).reshape(span_rows, heads_here, KEY_CHANNELS) / GATE_NORM
    bwd_log = (
        jax.nn.log_sigmoid(bwd_decay[::-1]).reshape(span_rows, heads_here, KEY_CHANNELS) / GATE_NORM
    )
    query_back = query_rows[::-1]
    key_back = key_data[::-1]
    value_back = value_matrix[::-1]
    fwd_summary = summarize(key_data, value_matrix, fwd_log)
    bwd_summary = summarize(key_back, value_back, bwd_log)
    fwd_carry, bwd_carry = carried_in(fwd_summary, bwd_summary, "sp")
    fwd_out, _ = blockwise(query_rows, key_data, value_matrix, fwd_log, fwd_carry)
    bwd_out, _ = blockwise(query_back, key_back, value_back, bwd_log, bwd_carry)
    combined = normalize(fwd_out + bwd_out[::-1]) * head_gain.reshape(heads_here, DV)
    head_mixed = (
        combined.reshape(span_rows, -1) * jax.nn.silu(out_gate.astype(jnp.float32))
    ).astype(jnp.bfloat16)
    mixed_out = lax.all_to_all(head_mixed, "tp", split_axis=0, concat_axis=1, tiled=True)
    projected = jnp.dot(mixed_out, out_proj, preferred_element_type=jnp.float32)
    residual = (stream.astype(jnp.float32) + normalize(projected) * mix_gain).astype(jnp.bfloat16)
    normed = (normalize(residual.astype(jnp.float32)) * ffn_gain).astype(jnp.bfloat16)
    model_width = normed.shape[1]
    outgoing = lax.dot_general(
        pick, normed, (((0,), (0,)), ((), ())), preferred_element_type=jnp.float32
    ).astype(jnp.bfloat16)
    arrived = lax.all_to_all(
        outgoing.reshape(experts, capacity, model_width),
        "sp",
        split_axis=0,
        concat_axis=0,
        tiled=True,
    )
    shared_sum = feed_forward(normed, shared_gate_parts, shared_up_parts, shared_down_mat)
    routed_done = feed_forward(
        arrived.reshape(experts * capacity, model_width), gate_parts, up_parts, down_mat
    ).astype(jnp.bfloat16)
    routed_back = lax.all_to_all(
        routed_done.reshape(experts, capacity, model_width),
        "sp",
        split_axis=0,
        concat_axis=0,
        tiled=True,
    ).reshape(experts * capacity, model_width)
    mixture = (
        shared_sum
        + jnp.dot(weights_high, routed_back, preferred_element_type=jnp.float32)
        + jnp.dot(weights_low, routed_back, preferred_element_type=jnp.float32)
    )
    return (residual.astype(jnp.float32) + normalize(mixture) * moe_gain).astype(jnp.bfloat16)


def solution(mesh):
    return jax.shard_map(
        body,
        mesh=mesh,
        in_specs=(
            P(("sp", "tp"), None),
            P("sp", "tp"),
            P("sp", "tp"),
            P("sp", "tp"),
            P("sp", "tp"),
            P("sp", "tp"),
            P("sp", "tp"),
            P("tp"),
            P(),
            P(),
            P(),
            P(),
            P(("sp", "tp"), None),
            P(("sp", "tp"), None),
            P("sp", None, "tp"),
            P("sp", None, "tp"),
            P("sp", "tp", None),
            P(None, "tp"),
            P(None, "tp"),
            P("tp", None),
        ),
        out_specs=P(("sp", "tp"), None),
        check_vma=False,
    )
```

time: 541 us -> 288 us (0.53); the launches traced: 532 us -> 286 us
  blocking collectives: 141 us -> 33.1 us
  waiting for transfers between devices: 150 us -> 66.7 us
  local copies, waits for them, and re-layouts: 102 us -> 42.4 us
  matrix products: 61.4 us -> 83 us
  other arithmetic: 52.3 us -> 32.2 us
    reduce_scatter x1 -> x0, waiting for transfers between devices: 71.5 us -> none  [body(): lax.psum_scatter(jnp.concatenate([routed_out, shared_out], axis=1).reshap...]
    all_gather x4 -> x1, blocking collectives: 101 us -> 33.1 us  [carried_in(): gathered = lax.all_gather(packed, axis).astype(jnp.float32)]
    all_to_all x1 -> x0, blocking collectives: 40.1 us -> none  [body(): lax.all_to_all(fill_slots(normed, routes, experts, capacity), 'sp', split...]
    all_gather x2 -> x6, waiting for transfers between devices: 37.3 us -> 0.06 us  [the longest x1 0.02 us: body(): shared_gate_parts = lax.all_gather(shared_gate, 'tp')]
    scatter x1 -> x0, local copies, waits for them, and re-layouts: 33.4 us -> none  [fill_slots(): return buffer.at[flat_ids, slot_ids].set(row_data[token_ids])]
    dynamic_slice x32 -> x0, local copies, waits for them, and re-layouts: 32 us -> none  [blockwise(): lax.scan(advance, start_state, (query_in, key_out, value_blocks, block_de...]
    dot_general x5 -> x20, matrix products: 19.1 us -> 44.4 us  [the longest x8 32.3 us: feed_forward(): jnp.dot(hidden, down_mat[group * width:(group + 1) * width], preferred_el...]
    all_to_all x1 -> x2, waiting for transfers between devices: 36.7 us -> 58.7 us  [the longest x1 36.1 us: body(): lax.all_to_all(outgoing.reshape(experts, capacity, model_width), 'sp', sp...]
  transfers between devices with their start and end apart: 5 -> 9, of which waited for: 4 -> 3; matrix products, arithmetic and copies ran while one was open for 8% -> 54% of each run, Pallas kernels for 0% -> 0%
where the time goes in v1:
time: 288 us; the launch traced here: 286 us
  matrix products  83 us (29%)
  waiting for transfers between devices  66.7 us (23%)
  local copies, waits for them, and re-layouts  42.4 us (15%)
  blocking collectives  33.1 us (11%)
  other arithmetic  32.2 us (11%)
  between operations  15.1 us (5%)
  starting transfers between devices  13.4 us (5%)
    all_to_all x1, waiting for transfers between devices, body(): lax.all_to_all(outgoing.reshape(experts, capacity, model_width), 'sp', sp...  36.1 us
    all_gather x1, blocking collectives, carried_in(): gathered = lax.all_gather(packed, axis).astype(jnp.float32)  33.1 us
    dot_general x8, matrix products, feed_forward(): jnp.dot(hidden, down_mat[group * width:(group + 1) * width], preferred_el...  32.3 us
    all_to_all x1, waiting for transfers between devices, body(): lax.all_to_all(routed_done.reshape(experts, capacity, model_width), 'sp',...  22.5 us
    dot_general x16, matrix products, advance(): jnp.einsum('asu,sun->asn', query_segment, carried_state, precision=TOP_PR...  17.6 us
    another operation x2, other arithmetic, blockwise(): jnp.cumsum(log_decay.reshape(block_count, BLK, head_count, key_width), ax...  14.1 us
    dot_general x14, matrix products, advance(): jnp.einsum('jco,jcm->com', key_segment, value_segment, precision=TOP_PREC...  10.9 us
    slice x17, local copies, waits for them, and re-layouts, blockwise(): lax.scan(advance, start_state, (query_in, key_out, value_blocks, block_de...  9.6 us
  transfers between devices with their start and end apart: 9, of which 3 were waited for; matrix products, arithmetic and copies ran while one was open for 54% of the time, Pallas kernels for 0%

profile of v1, /device:TPU:0, one launch (start us, length us, event | category | flops | bytes accessed | tf_op | source)
XLA Modules:
  0.0 286.0 jit_solution(18210130579138707508)
XLA Ops:
  11.9 2.4 reduce-window.14
  17.0 2.4 reduce-window.16
  22.3 3.8 %rev.17 = f32[512,2,128]{0,2,1:T(8,128)S(1)} reverse(f32[512,2,128]{0,2,1:T(8,128)} %bitcast.614), dimensions={0} | reverse | bytes 1048576 | tf_op jit(solution)/shard_map/rev | solution.py:197
  26.1 1.3 fusion.30
  29.0 33.1 %all_gather.28 = bf16[8,258,128]{2,1,0:T(8,128)(2,1)S(1)} all-gather(bf16[1,258,128]{2,1,0:T(8,128)(2,1)S(1)} %pad_maximum_fusion.2), channel_id=1, replica_groups=mesh['sp'=8,'tp'=4] {'sp'}, dimensions={0}, use_global_device_ids=true | all-gather | bytes 594432 | tf_op jit(solution)/shard_map/all_gather | solution.py:27
  62.1 1.0 slice.615
  63.2 1.0 copy.358
  64.2 1.1 fusion.217
  65.9 1.0 copy.380
  68.4 1.0 copy.359
  69.4 1.0 copy.378
  71.4 3.3 %rev.18 = f32[512,2,64]{0,2,1:T(8,128)} reverse(f32[512,2,64]{0,2,1:T(8,128)} %get-tuple-element.71), dimensions={0} | reverse | bytes 524288 | tf_op jit(solution)/shard_map/rev | solution.py:195
  75.1 13.0 %fusion.218 = f32[8,64,2,64]{3,0,1,2:T(8,128)S(1)} fusion(f32[8,64,2,64]{3,0,1,2:T(8,128)S(1)} %copy.390), kind=kOutput, calls=%fused_computation.394 | output fusion | flops 4128768 | bytes 524288 | tf_op jit(solution)/shard_map/jit(cumsum)/reduce_window_sum | solution.py:69
  88.8 1.0 copy.400
  91.4 1.0 copy.361
  93.1 1.4 fusion.190
  94.5 1.3 copy.379
  95.8 1.6 fusion.215
  99.2 1.6 fusion.216
  105.2 1.0 copy.398
  106.2 1.3 fusion.65
  107.6 2.2 copy_multiply_fusion.1
  110.2 1.1 fusion.24
  112.3 1.0 fusion.23
  113.4 1.0 convolution_add_fusion.17
  114.4 1.0 fusion.22
  116.5 1.0 fusion.21
  118.6 1.0 fusion.20
  120.7 1.0 fusion.19
  122.7 1.0 fusion.18
  124.9 1.1 fusion.17
  130.9 1.1 convolution_select_fusion.1
  132.0 1.2 fusion.1
  134.8 1.1 copy.389
  137.1 1.0 convolution_add_fusion.7
  138.2 1.7 fusion.11
  139.8 1.0 convolution_add_fusion.6
  140.9 1.7 fusion.10
  142.5 1.0 convolution_add_fusion.5
  143.6 1.7 fusion.9
  145.4 1.1 convolution_select_fusion
  146.5 1.7 fusion
  150.6 3.4 %all-to-all-start = ((bf16[4,128,256]{2,1,0:T(8,128)(2,1)}), bf16[4,128,256]{2,1,0:T(8,128)(2,1)S(1)}, u32[]{:S(2)}, u32[]{:S(2)}) async-start(bf16[4,128,256]{2,1,0:T(8,128)(2,1)} %bitcast.143), calls=%async_computation | async-start | bytes 524288 | tf_op jit(solution)/shard_map/all_to_all | solution.py:207
  155.5 4.6 %all-to-all-done = bf16[4,128,256]{2,1,0:T(8,128)(2,1)S(1)} async-done(((bf16[4,128,256]{2,1,0:T(8,128)(2,1)}), bf16[4,128,256]{2,1,0:T(8,128)(2,1)S(1)}, u32[]{:S(2)}, u32[]{:S(2)}) %all-to-all-start) | async-done | bytes 262176 | tf_op jit(solution)/shard_map/all_to_all | solution.py:207
  160.2 3.1 %multiply_reduce_fusion.1 = (f32[128]{0:T(128)S(1)}, f32[128,2048]{1,0:T(8,128)S(1)}) fusion(bf16[128,1024]{0,1:T(8,128)(2,1)S(1)} %bitcast.616, bf16[1024,2048]{1,0:T(8,128)(2,1)} %param.28), kind=kOutput, calls=%fused_computation.110 | convolution fusion | flops 537395072 | bytes 5505536 | tf_op jit(solution)/shard_map/dot_general | solution.py:208
  164.0 1.8 convolution_convert_fusion
  165.8 5.6 %all-to-all-start.1 = ((bf16[8,48,2048]{2,1,0:T(8,128)(2,1)}), bf16[8,48,2048]{2,1,0:T(8,128)(2,1)S(1)}, u32[]{:S(2)}, u32[]{:S(2)}) async-start(bf16[8,48,2048]{2,1,0:T(8,128)(2,1)} %bitcast.608), calls=%async_computation.1 | async-start | bytes 3145728 | tf_op jit(solution)/shard_map/all_to_all | solution.py:215
  172.0 36.1 %all-to-all-done.1 = bf16[8,48,2048]{2,1,0:T(8,128)(2,1)S(1)} async-done(((bf16[8,48,2048]{2,1,0:T(8,128)(2,1)}), bf16[8,48,2048]{2,1,0:T(8,128)(2,1)S(1)}, u32[]{:S(2)}, u32[]{:S(2)}) %all-to-all-start.1) | async-done | bytes 1572896 | tf_op jit(solution)/shard_map/all_to_all | solution.py:215
  208.1 1.9 fusion.39
  211.9 5.0 %fusion.7 = f32[384,2048]{1,0:T(8,128)} fusion(bf16[384,2048]{1,0:T(8,128)(2,1)S(1)} %bitcast.600, bf16[1,1024,2048]{2,1,0:T(8,128)(2,1)} %all-gather.20.cloned.1.call-done, bf16[4,2048,256]{2,1,0:T(8,128)(2,1)} %all-gather.14.cloned.1.call-done, f32[384,256]{1,0:T(8,128)S(1)} %fusion.39), kind=kOutput, calls=%fused_computation.25 | convolution fusion | flops 805896192 | bytes 7208960 | tf_op jit(solution)/shard_map/dot_general | solution.py:119
  216.8 1.8 fusion.37
  218.6 5.0 %fusion.8 = f32[384,2048]{1,0:T(8,128)} fusion(bf16[384,2048]{1,0:T(8,128)(2,1)S(1)} %bitcast.602, bf16[1,1024,2048]{2,1,0:T(8,128)(2,1)} %all-gather.20.cloned.1.call-done, bf16[4,2048,256]{2,1,0:T(8,128)(2,1)} %all-gather.14.cloned.1.call-done, f32[384,256]{1,0:T(8,128)S(1)} %fusion.40), kind=kOutput, calls=%fused_computation.26 | convolution fusion | flops 805896192 | bytes 7208960 | tf_op jit(solution)/shard_map/dot_general | solution.py:119
  223.7 5.0 %fusion.6 = f32[384,2048]{1,0:T(8,128)} fusion(bf16[384,2048]{1,0:T(8,128)(2,1)S(1)} %bitcast.603, bf16[1,1024,2048]{2,1,0:T(8,128)(2,1)} %all-gather.20.cloned.1.call-done, bf16[4,2048,256]{2,1,0:T(8,128)(2,1)} %all-gather.14.cloned.1.call-done, f32[384,256]{1,0:T(8,128)S(1)} %fusion.38), kind=kOutput, calls=%fused_computation.24 | convolution fusion | flops 805896192 | bytes 7208960 | tf_op jit(solution)/shard_map/dot_general | solution.py:119
  228.6 7.3 %add_convert_fusion = bf16[384,2048]{1,0:T(8,128)(2,1)} fusion(f32[384,2048]{1,0:T(8,128)} %fusion.6, f32[384,2048]{1,0:T(8,128)} %fusion.8, f32[384,2048]{1,0:T(8,128)} %fusion.7, bf16[1,1024,2048]{2,1,0:T(8,128)(2,1)} %all-gather.20.cloned.1.call-done, bf16[384,2048]{1,0:T(8,128)(2,1)S(1)} %bitcast.604, ...), kind=kOutput, calls=%fused_computation | convolution fusion | flops 809041920 | bytes 15073280 | tf_op jit(solution)/shard_map/dot_general | solution.py:119
  236.0 4.0 %all-to-all-start.2 = ((bf16[8,48,2048]{2,1,0:T(8,128)(2,1)}), bf16[8,48,2048]{2,1,0:T(8,128)(2,1)S(1)}, u32[]{:S(2)}, u32[]{:S(2)}) async-start(bf16[8,48,2048]{2,1,0:T(8,128)(2,1)} %bitcast.607), calls=%async_computation.2 | async-start | bytes 3145728 | tf_op jit(solution)/shard_map/all_to_all | solution.py:226
  240.1 1.5 fusion.48
  241.7 1.4 fusion.53
  243.5 1.0 fusion.63
  244.5 1.8 fusion.31
  246.3 2.8 convolution_add_fusion.4
  249.1 3.2 %convolution_add_fusion.3 = f32[128,2048]{1,0:T(8,128)} fusion(f32[128,2048]{1,0:T(8,128)} %convolution_add_fusion.4, bf16[512,2048]{1,0:T(8,128)(2,1)} %all-gather.10.cloned.1.call-done, bf16[8192,128]{1,0:T(8,128)(2,1)} %all-gather.18.cloned.1.call-done, f32[128,128]{1,0:T(8,128)S(1)} %fusion.53, bf16[128,2048]{1,0:T(8,128)(2,1)S(1)} %get-tuple-element.6, ...), kind=kOutput, calls=%fused_computation.5 | convolution fusion | flops 135626752 | bytes 3744256 | tf_op jit(solution)/shard_map/dot_general | solution.py:119
  252.3 2.1 convolution_add_fusion.2
  254.4 22.5 %all-to-all-done.2 = bf16[8,48,2048]{2,1,0:T(8,128)(2,1)S(1)} async-done(((bf16[8,48,2048]{2,1,0:T(8,128)(2,1)}), bf16[8,48,2048]{2,1,0:T(8,128)(2,1)S(1)}, u32[]{:S(2)}, u32[]{:S(2)}) %all-to-all-start.2) | async-done | bytes 1572896 | tf_op jit(solution)/shard_map/all_to_all | solution.py:226
  278.1 1.0 fusion.36
  (289 shorter events, 47.1 us)
Async XLA Ops:
  6.5 201.6 %all-gather.12.cloned.1.call-start = ((), (), s32[]{:S(2)}) async-start(), calls=%async_computation.4 | async-start | bytes 5242880 | tf_op jit(solution)/shard_map/all_gather | solution.py:167
  7.3 204.6 %all-gather.14.cloned.1.call-start = ((), (), s32[]{:S(2)}) async-start(), calls=%async_computation.5 | async-start | bytes 5242880 | tf_op jit(solution)/shard_map/all_gather | solution.py:168
  8.0 203.8 %all-gather.20.cloned.1.call-start = ((), (), s32[]{:S(2)}) async-start(), calls=%async_computation.8 | async-start | bytes 5242880 | tf_op jit(solution)/shard_map/all_gather | solution.py:169
  8.7 231.4 %all-gather.16.cloned.1.call-start = ((), (), s32[]{:S(2)}) async-start(), calls=%async_computation.6 | async-start | bytes 2621440 | tf_op jit(solution)/shard_map/all_gather | solution.py:170
  11.4 4.8 %copy-start.17 = (f32[512,128]{1,0:T(8,128)S(1)}, f32[512,128]{1,0:T(8,128)}, u32[]{:S(2)}) copy-start(f32[512,128]{1,0:T(8,128)} %param.26) | copy-start | bytes 786436
  15.5 5.8 %copy-start.2 = (bf16[512,256]{1,0:T(8,128)(2,1)S(1)}, bf16[512,256]{1,0:T(8,128)(2,1)}, u32[]{:S(2)}) copy-start(bf16[512,256]{1,0:T(8,128)(2,1)} %param.23) | copy-start | bytes 786436
  21.3 6.8 %copy-start.70 = (bf16[2,64]{1,0:T(2,128)(2,1)S(1)}, bf16[2,64]{1,0:T(2,128)(2,1)}, u32[]{:S(2)}) copy-start(bf16[2,64]{1,0:T(2,128)(2,1)} %fusion.168) | copy-start | bytes 772
  21.3 6.9 %copy-start.36 = (f32[2,64]{1,0:T(2,128)S(1)}, f32[2,64]{1,0:T(2,128)}, u32[]{:S(2)}) copy-start(f32[2,64]{1,0:T(2,128)} %slice_reduce_fusion) | copy-start | bytes 1540
  63.2 5.1 %copy-start.1 = (f32[512,2,64]{0,2,1:T(8,128)S(1)}, f32[512,2,64]{0,2,1:T(8,128)}, u32[]{:S(2)}) copy-start(f32[512,2,64]{0,2,1:T(8,128)} %get-tuple-element.71) | copy-start | bytes 786436
  65.9 4.5 %copy-start.3 = (bf16[512,256]{1,0:T(8,128)(2,1)S(1)}, bf16[512,256]{1,0:T(8,128)(2,1)}, u32[]{:S(2)}) copy-start(bf16[512,256]{1,0:T(8,128)(2,1)} %param.23) | copy-start | bytes 786436
  88.1 9.2 %copy-start.8 = (f32[8,64,2,64]{3,1,2,0:T(8,128)S(1)}, f32[8,64,2,64]{3,1,2,0:T(8,128)}, u32[]{:S(2)}) copy-start(f32[8,64,2,64]{3,1,2,0:T(8,128)} %copy.378) | copy-start | bytes 786436
  91.4 7.0 %copy-start.11 = (f32[512,2,64]{0,2,1:T(8,128)S(1)}, f32[512,2,64]{0,2,1:T(8,128)}, u32[]{:S(2)}) copy-start(f32[512,2,64]{0,2,1:T(8,128)} %rev.18) | copy-start | bytes 786436
  98.4 9.1 %copy-start.31 = (f32[8,2,64]{2,1,0:T(2,128)S(1)}, f32[8,2,64]{2,1,0:T(2,128)}, u32[]{:S(2)}) copy-start(f32[8,2,64]{2,1,0:T(2,128)} %copy.379) | copy-start | bytes 12292
  105.1 4.8 %copy-start.60 = (f32[2,64]{1,0:T(2,128)S(1)}, f32[2,64]{1,0:T(2,128)}, u32[]{:S(2)}) copy-start(f32[2,64]{1,0:T(2,128)} %get-tuple-element.35) | copy-start | bytes 1540
  105.1 4.8 %copy-start.61 = (f32[2,64]{1,0:T(2,128)S(1)}, f32[2,64]{1,0:T(2,128)}, u32[]{:S(2)}) copy-start(f32[2,64]{1,0:T(2,128)} %get-tuple-element.44) | copy-start | bytes 1540
  105.1 4.8 %copy-start.62 = (f32[2,64]{1,0:T(2,128)S(1)}, f32[2,64]{1,0:T(2,128)}, u32[]{:S(2)}) copy-start(f32[2,64]{1,0:T(2,128)} %get-tuple-element.45) | copy-start | bytes 1540
  105.1 4.8 %copy-start.63 = (f32[2,64]{1,0:T(2,128)S(1)}, f32[2,64]{1,0:T(2,128)}, u32[]{:S(2)}) copy-start(f32[2,64]{1,0:T(2,128)} %get-tuple-element.46) | copy-start | bytes 1540
  105.1 4.8 %copy-start.64 = (f32[2,64]{1,0:T(2,128)S(1)}, f32[2,64]{1,0:T(2,128)}, u32[]{:S(2)}) copy-start(f32[2,64]{1,0:T(2,128)} %get-tuple-element.47) | copy-start | bytes 1540
  105.1 4.8 %copy-start.65 = (f32[2,64]{1,0:T(2,128)S(1)}, f32[2,64]{1,0:T(2,128)}, u32[]{:S(2)}) copy-start(f32[2,64]{1,0:T(2,128)} %get-tuple-element.48) | copy-start | bytes 1540
  105.1 4.8 %copy-start.66 = (f32[2,64]{1,0:T(2,128)S(1)}, f32[2,64]{1,0:T(2,128)}, u32[]{:S(2)}) copy-start(f32[2,64]{1,0:T(2,128)} %get-tuple-element.49) | copy-start | bytes 1540
  105.2 4.8 %copy-start.67 = (f32[2,64]{1,0:T(2,128)S(1)}, f32[2,64]{1,0:T(2,128)}, u32[]{:S(2)}) copy-start(f32[2,64]{1,0:T(2,128)} %get-tuple-element.50) | copy-start | bytes 1540
  106.2 5.1 %copy-start.28 = (bf16[8,2,8,128]{3,2,1,0:T(8,128)(2,1)S(1)}, bf16[8,2,8,128]{3,2,1,0:T(8,128)(2,1)}, u32[]{:S(2)}) copy-start(bf16[8,2,8,128]{3,2,1,0:T(8,128)(2,1)} %get-tuple-element.24) | copy-start | bytes 98308
  106.2 5.1 %copy-start.50 = (f32[1,2,64]{2,0,1:T(1,128)S(1)}, f32[1,2,64]{2,0,1:T(1,128)}, u32[]{:S(2)}) copy-start(f32[1,2,64]{2,0,1:T(1,128)} %get-tuple-element.57) | copy-start | bytes 1540
  106.2 7.2 %copy-start.27 = (bf16[8,2,8,128]{3,2,1,0:T(8,128)(2,1)S(1)}, bf16[8,2,8,128]{3,2,1,0:T(8,128)(2,1)}, u32[]{:S(2)}) copy-start(bf16[8,2,8,128]{3,2,1,0:T(8,128)(2,1)} %get-tuple-element.23) | copy-start | bytes 98308
  106.2 7.2 %copy-start.49 = (f32[1,2,64]{2,0,1:T(1,128)S(1)}, f32[1,2,64]{2,0,1:T(1,128)}, u32[]{:S(2)}) copy-start(f32[1,2,64]{2,0,1:T(1,128)} %get-tuple-element.56) | copy-start | bytes 1540
  106.2 9.2 %copy-start.26 = (bf16[8,2,8,128]{3,2,1,0:T(8,128)(2,1)S(1)}, bf16[8,2,8,128]{3,2,1,0:T(8,128)(2,1)}, u32[]{:S(2)}) copy-start(bf16[8,2,8,128]{3,2,1,0:T(8,128)(2,1)} %get-tuple-element.22) | copy-start | bytes 98308
  106.2 9.2 %copy-start.48 = (f32[1,2,64]{2,0,1:T(1,128)S(1)}, f32[1,2,64]{2,0,1:T(1,128)}, u32[]{:S(2)}) copy-start(f32[1,2,64]{2,0,1:T(1,128)} %get-tuple-element.55) | copy-start | bytes 1540
  107.5 25.7 %copy-start.4 = (f32[8,64,2,64]{3,1,2,0:T(8,128)}, f32[8,64,2,64]{3,1,2,0:T(8,128)S(1)}, u32[]{:S(2)}) copy-start(f32[8,64,2,64]{3,1,2,0:T(8,128)S(1)} %fusion.65) | copy-start | bytes 786436
  107.5 10.0 %copy-start.25 = (bf16[8,2,8,128]{3,2,1,0:T(8,128)(2,1)S(1)}, bf16[8,2,8,128]{3,2,1,0:T(8,128)(2,1)}, u32[]{:S(2)}) copy-start(bf16[8,2,8,128]{3,2,1,0:T(8,128)(2,1)} %get-tuple-element.21) | copy-start | bytes 98308
  107.5 10.0 %copy-start.47 = (f32[1,2,64]{2,0,1:T(1,128)S(1)}, f32[1,2,64]{2,0,1:T(1,128)}, u32[]{:S(2)}) copy-start(f32[1,2,64]{2,0,1:T(1,128)} %get-tuple-element.54) | copy-start | bytes 1540
  107.5 12.1 %copy-start.24 = (bf16[8,2,8,128]{3,2,1,0:T(8,128)(2,1)S(1)}, bf16[8,2,8,128]{3,2,1,0:T(8,128)(2,1)}, u32[]{:S(2)}) copy-start(bf16[8,2,8,128]{3,2,1,0:T(8,128)(2,1)} %get-tuple-element.20) | copy-start | bytes 98308
  107.6 12.1 %copy-start.46 = (f32[1,2,64]{2,0,1:T(1,128)S(1)}, f32[1,2,64]{2,0,1:T(1,128)}, u32[]{:S(2)}) copy-start(f32[1,2,64]{2,0,1:T(1,128)} %get-tuple-element.53) | copy-start | bytes 1540
  107.6 14.2 %copy-start.23 = (bf16[8,2,8,128]{3,2,1,0:T(8,128)(2,1)S(1)}, bf16[8,2,8,128]{3,2,1,0:T(8,128)(2,1)}, u32[]{:S(2)}) copy-start(bf16[8,2,8,128]{3,2,1,0:T(8,128)(2,1)} %get-tuple-element.25) | copy-start | bytes 98308
  107.6 14.2 %copy-start.45 = (f32[1,2,64]{2,0,1:T(1,128)S(1)}, f32[1,2,64]{2,0,1:T(1,128)}, u32[]{:S(2)}) copy-start(f32[1,2,64]{2,0,1:T(1,128)} %get-tuple-element.52) | copy-start | bytes 1540
  109.8 14.0 %copy-start.22 = (bf16[8,2,8,128]{3,2,1,0:T(8,128)(2,1)S(1)}, bf16[8,2,8,128]{3,2,1,0:T(8,128)(2,1)}, u32[]{:S(2)}) copy-start(bf16[8,2,8,128]{3,2,1,0:T(8,128)(2,1)} %get-tuple-element.19) | copy-start | bytes 98308
  109.8 14.0 %copy-start.44 = (f32[1,2,64]{2,0,1:T(1,128)S(1)}, f32[1,2,64]{2,0,1:T(1,128)}, u32[]{:S(2)}) copy-start(f32[1,2,64]{2,0,1:T(1,128)} %get-tuple-element.51) | copy-start | bytes 1540
  109.8 16.2 %copy-start.52 = (f32[2,64]{1,0:T(2,128)S(1)}, f32[2,64]{1,0:T(2,128)}, u32[]{:S(2)}) copy-start(f32[2,64]{1,0:T(2,128)} %get-tuple-element.36) | copy-start | bytes 1540
  109.8 16.2 %copy-start.53 = (f32[2,64]{1,0:T(2,128)S(1)}, f32[2,64]{1,0:T(2,128)}, u32[]{:S(2)}) copy-start(f32[2,64]{1,0:T(2,128)} %get-tuple-element.37) | copy-start | bytes 1540
  109.8 16.2 %copy-start.54 = (f32[2,64]{1,0:T(2,128)S(1)}, f32[2,64]{1,0:T(2,128)}, u32[]{:S(2)}) copy-start(f32[2,64]{1,0:T(2,128)} %get-tuple-element.38) | copy-start | bytes 1540
  109.8 16.2 %copy-start.55 = (f32[2,64]{1,0:T(2,128)S(1)}, f32[2,64]{1,0:T(2,128)}, u32[]{:S(2)}) copy-start(f32[2,64]{1,0:T(2,128)} %get-tuple-element.39) | copy-start | bytes 1540
  109.8 16.2 %copy-start.56 = (f32[2,64]{1,0:T(2,128)S(1)}, f32[2,64]{1,0:T(2,128)}, u32[]{:S(2)}) copy-start(f32[2,64]{1,0:T(2,128)} %get-tuple-element.40) | copy-start | bytes 1540
  109.9 16.2 %copy-start.57 = (f32[2,64]{1,0:T(2,128)S(1)}, f32[2,64]{1,0:T(2,128)}, u32[]{:S(2)}) copy-start(f32[2,64]{1,0:T(2,128)} %get-tuple-element.41) | copy-start | bytes 1540
  109.9 16.2 %copy-start.58 = (f32[2,64]{1,0:T(2,128)S(1)}, f32[2,64]{1,0:T(2,128)}, u32[]{:S(2)}) copy-start(f32[2,64]{1,0:T(2,128)} %get-tuple-element.42) | copy-start | bytes 1540
  109.9 16.2 %copy-start.59 = (f32[2,64]{1,0:T(2,128)S(1)}, f32[2,64]{1,0:T(2,128)}, u32[]{:S(2)}) copy-start(f32[2,64]{1,0:T(2,128)} %get-tuple-element.43) | copy-start | bytes 1540
  110.2 16.9 %copy-start.7 = (f32[8,64,2,64]{1,3,2,0:T(8,128)S(1)}, f32[8,64,2,64]{1,3,2,0:T(8,128)}, u32[]{:S(2)}) copy-start(f32[8,64,2,64]{1,3,2,0:T(8,128)} %copy.400) | copy-start | bytes 786436
  117.5 9.8 %copy-start.20 = (f32[64,2,128]{2,0,1:T(8,128)S(1)}, f32[64,2,128]{2,0,1:T(8,128)}, u32[]{:S(2)}) copy-start(f32[64,2,128]{2,0,1:T(8,128)} %slice.528) | copy-start | bytes 196612
  117.5 9.8 %copy-start.43 = (f32[1,2,64]{2,0,1:T(1,128)S(1)}, f32[1,2,64]{2,0,1:T(1,128)}, u32[]{:S(2)}) copy-start(f32[1,2,64]{2,0,1:T(1,128)} %get-tuple-element.64) | copy-start | bytes 1540
  119.6 8.8 %copy-start.19 = (f32[64,2,128]{2,0,1:T(8,128)S(1)}, f32[64,2,128]{2,0,1:T(8,128)}, u32[]{:S(2)}) copy-start(f32[64,2,128]{2,0,1:T(8,128)} %slice.534) | copy-start | bytes 196612
  119.6 8.8 %copy-start.42 = (f32[1,2,64]{2,0,1:T(1,128)S(1)}, f32[1,2,64]{2,0,1:T(1,128)}, u32[]{:S(2)}) copy-start(f32[1,2,64]{2,0,1:T(1,128)} %get-tuple-element.63) | copy-start | bytes 1540
  121.7 7.7 %copy-start.41 = (f32[1,2,64]{2,0,1:T(1,128)S(1)}, f32[1,2,64]{2,0,1:T(1,128)}, u32[]{:S(2)}) copy-start(f32[1,2,64]{2,0,1:T(1,128)} %get-tuple-element.62) | copy-start | bytes 1540
  123.8 6.7 %copy-start.40 = (f32[1,2,64]{2,0,1:T(1,128)S(1)}, f32[1,2,64]{2,0,1:T(1,128)}, u32[]{:S(2)}) copy-start(f32[1,2,64]{2,0,1:T(1,128)} %get-tuple-element.61) | copy-start | bytes 1540
  124.8 5.9 %copy-start.5 = (f32[8,64,2,64]{3,0,1,2:T(8,128)S(1)}, f32[8,64,2,64]{3,0,1,2:T(8,128)}, u32[]{:S(2)}) copy-start(f32[8,64,2,64]{3,0,1,2:T(8,128)} %copy.359) | copy-start | bytes 786436
  124.8 5.9 %copy-start.6 = (f32[8,64,2,64]{3,0,1,2:T(8,128)S(1)}, f32[8,64,2,64]{3,0,1,2:T(8,128)}, u32[]{:S(2)}) copy-start(f32[8,64,2,64]{3,0,1,2:T(8,128)} %copy.361) | copy-start | bytes 786436
  124.8 5.9 %copy-start.33 = (f32[8,2,64]{2,0,1:T(8,128)S(1)}, f32[8,2,64]{2,0,1:T(8,128)}, u32[]{:S(2)}) copy-start(f32[8,2,64]{2,0,1:T(8,128)} %get-tuple-element.11) | copy-start | bytes 12292
  134.3 5.5 %copy-start.38 = (f32[1,2,64]{2,0,1:T(1,128)S(1)}, f32[1,2,64]{2,0,1:T(1,128)}, u32[]{:S(2)}) copy-start(f32[1,2,64]{2,0,1:T(1,128)} %get-tuple-element.59) | copy-start | bytes 1540
  134.6 8.0 %copy-start.37 = (f32[1,2,64]{2,0,1:T(1,128)S(1)}, f32[1,2,64]{2,0,1:T(1,128)}, u32[]{:S(2)}) copy-start(f32[1,2,64]{2,0,1:T(1,128)} %get-tuple-element.58) | copy-start | bytes 1540
  134.6 10.7 %copy-start.32 = (f32[8,2,64]{2,0,1:T(8,128)S(1)}, f32[8,2,64]{2,0,1:T(8,128)}, u32[]{:S(2)}) copy-start(f32[8,2,64]{2,0,1:T(8,128)} %get-tuple-element.13) | copy-start | bytes 12292
  149.1 5.6 %copy-start.51 = (s32[128,2]{0,1:T(2,128)S(1)}, s32[128,2]{0,1:T(2,128)}, u32[]{:S(2)}) copy-start(s32[128,2]{0,1:T(2,128)} %param.32) | copy-start | bytes 3076
  150.6 9.4 %all-to-all-start = ((bf16[4,128,256]{2,1,0:T(8,128)(2,1)}), bf16[4,128,256]{2,1,0:T(8,128)(2,1)S(1)}, u32[]{:S(2)}, u32[]{:S(2)}) async-start(bf16[4,128,256]{2,1,0:T(8,128)(2,1)} %bitcast.143), calls=%async_computation | async-start | bytes 524288 | tf_op jit(solution)/shard_map/all_to_all | solution.py:207
  154.0 90.4 %all-gather.10.cloned.1.call-start = ((), (), s32[]{:S(2)}) async-start(), calls=%async_computation.3 | async-start | bytes 2621440 | tf_op jit(solution)/shard_map/all_gather | solution.py:172
  165.8 42.3 %all-to-all-start.1 = ((bf16[8,48,2048]{2,1,0:T(8,128)(2,1)}), bf16[8,48,2048]{2,1,0:T(8,128)(2,1)S(1)}, u32[]{:S(2)}, u32[]{:S(2)}) async-start(bf16[8,48,2048]{2,1,0:T(8,128)(2,1)} %bitcast.608), calls=%async_computation.1 | async-start | bytes 3145728 | tf_op jit(solution)/shard_map/all_to_all | solution.py:215
  171.4 73.0 %all-gather.18.cloned.1.call-start = ((), (), s32[]{:S(2)}) async-start(), calls=%async_computation.7 | async-start | bytes 2621440 | tf_op jit(solution)/shard_map/all_gather | solution.py:171
  236.0 4.0 %copy-start.68 = (f32[128,2]{0,1:T(2,128)S(1)}, f32[128,2]{0,1:T(2,128)}, u32[]{:S(2)}) copy-start(f32[128,2]{0,1:T(2,128)} %param.33) | copy-start | bytes 3076
  236.0 41.0 %all-to-all-start.2 = ((bf16[8,48,2048]{2,1,0:T(8,128)(2,1)}), bf16[8,48,2048]{2,1,0:T(8,128)(2,1)S(1)}, u32[]{:S(2)}, u32[]{:S(2)}) async-start(bf16[8,48,2048]{2,1,0:T(8,128)(2,1)} %bitcast.607), calls=%async_computation.2 | async-start | bytes 3145728 | tf_op jit(solution)/shard_map/all_to_all | solution.py:226
  (18 other events, 40.0 us)
Sparse Core Ops, SparseCore 0:
  8.9 37.2 all-gather.11
  47.7 34.4 all-gather.13
  83.7 34.4 all-gather.19
  119.6 22.5 all-gather.15
  156.1 24.0 all-gather.9
  181.6 22.5 all-gather.17

commit v2 on v1

v2 whole, which is shorter than its diff:
```python
import functools

import jax
import jax.numpy as jnp
from jax import lax
from jax.experimental import pallas as pl
from jax.experimental.pallas import tpu as pltpu
from jax.sharding import PartitionSpec as P

KEY_CHANNELS = 64
DV = 128
BLK = 64
TOPK = 2


EPS = 1e-06
GATE_NORM = 16.0
ROPE_BASE = 10000.0
TOP_PRECISION = lax.Precision.HIGHEST
MESH = pl.DeviceIdType.MESH


def normalize(tensor):
    return tensor * lax.rsqrt(jnp.mean(tensor * tensor, axis=-1, keepdims=True) + EPS)


def dot_nt(left, right):
    return lax.dot_general(
        left, right, (((1,), (1,)), ((), ())), preferred_element_type=jnp.float32
    )


def dot_tn(left, right):
    return lax.dot_general(
        left, right, (((0,), (0,)), ((), ())), preferred_element_type=jnp.float32
    )


def attention_kernel(
    sp_count,
    tp_count,
    q_ref,
    k_ref,
    v_ref,
    gate_ref,
    fwd_ref,
    bwd_ref,
    cos_ref,
    sin_ref,
    gain_ref,
    out_ref,
    own_ref,
    got_ref,
    mixed_ref,
    land_ref,
    within_ref,
    key_ref,
    sums_f,
    sums_b,
    sum_send,
    sum_recv,
    row_send,
    row_recv,
):
    span, lanes = q_ref.shape
    width = v_ref.shape[1]
    heads = lanes // KEY_CHANNELS
    blocks = span // BLK
    rows_out = span // tp_count
    sp_me = lax.axis_index("sp")
    tp_me = lax.axis_index("tp")

    barrier = pltpu.get_barrier_semaphore()
    for step in range(1, sp_count):
        pl.semaphore_signal(
            barrier,
            inc=1,
            device_id=(lax.rem(sp_me + step, sp_count), tp_me),
            device_id_type=MESH,
        )
    for step in range(1, tp_count):
        pl.semaphore_signal(
            barrier,
            inc=1,
            device_id=(sp_me, lax.rem(tp_me + step, tp_count)),
            device_id_type=MESH,
        )

    row = lax.broadcasted_iota(jnp.int32, (BLK, BLK), 0)
    column = lax.broadcasted_iota(jnp.int32, (BLK, BLK), 1)
    lower = row >= column
    upper = row <= column
    lower_ones = lower.astype(jnp.float32)
    upper_ones = upper.astype(jnp.float32)
    from_lane = lax.broadcasted_iota(jnp.int32, (lanes, lanes), 0)
    to_lane = lax.broadcasted_iota(jnp.int32, (lanes, lanes), 1)
    half = KEY_CHANNELS // 2
    partner = jnp.where(lax.rem(to_lane, KEY_CHANNELS) < half, to_lane + half, to_lane - half)
    swap = (from_lane == partner).astype(jnp.bfloat16)
    own_head = (
        lax.broadcasted_iota(jnp.int32, (width, lanes), 0) // DV
        == lax.broadcasted_iota(jnp.int32, (width, lanes), 1) // KEY_CHANNELS
    )
    lane_head = lax.broadcasted_iota(jnp.int32, (BLK, lanes), 1) // KEY_CHANNELS

    def rotated(tensor, rows):
        swapped = jnp.dot(tensor, swap, preferred_element_type=jnp.float32)
        return tensor.astype(jnp.float32) * cos_ref[rows, :] + swapped * sin_ref[rows, :]

    cumul_f, cumul_b, decay_f, decay_b = [], [], [], []
    for block in range(blocks):
        rows = pl.ds(block * BLK, BLK)
        total_f = jnp.dot(
            lower_ones, fwd_ref[rows, :], precision=TOP_PRECISION, preferred_element_type=jnp.float32
        )
        total_b = jnp.dot(
            upper_ones, bwd_ref[rows, :], precision=TOP_PRECISION, preferred_element_type=jnp.float32
        )
        last_f = total_f[BLK - 1 : BLK]
        last_b = total_b[0:1]
        keys = rotated(k_ref[rows, :], rows)
        key_ref[rows, :] = keys
        value_rows = v_ref[rows, :]
        out_f = (keys * jnp.exp(last_f - total_f)).astype(jnp.bfloat16)
        out_b = (keys * jnp.exp(last_b - total_b)).astype(jnp.bfloat16)
        sums_f[block] = jnp.where(own_head, dot_tn(value_rows, out_f), 0.0)
        sums_b[block] = jnp.where(own_head, dot_tn(value_rows, out_b), 0.0)
        cumul_f.append(total_f)
        cumul_b.append(total_b)
        decay_f.append(jnp.exp(last_f))
        decay_b.append(jnp.exp(last_b))

    def packed(total):
        return sum(total[h * DV : (h + 1) * DV] for h in range(heads))

    total = sums_f[0]
    through = decay_f[0]
    for block in range(1, blocks):
        total = total * decay_f[block] + sums_f[block]
        through = through * decay_f[block]
    own_ref[0:DV, :] = packed(total).astype(jnp.bfloat16)
    own_ref[2 * DV : 2 * DV + 8, :] = jnp.broadcast_to(through, (8, lanes)).astype(jnp.bfloat16)
    total = sums_b[blocks - 1]
    through = decay_b[blocks - 1]
    for block in range(blocks - 2, -1, -1):
        total = total * decay_b[block] + sums_b[block]
        through = through * decay_b[block]
    own_ref[DV : 2 * DV, :] = packed(total).astype(jnp.bfloat16)
    own_ref[2 * DV + 8 : 2 * DV + 16, :] = jnp.broadcast_to(through, (8, lanes)).astype(
        jnp.bfloat16
    )

    pl.semaphore_wait(barrier, sp_count - 1 + tp_count - 1)
    sum_copies = []
    for step in range(1, sp_count):
        copy = pltpu.make_async_remote_copy(
            src_ref=own_ref,
            dst_ref=got_ref.at[step],
            send_sem=sum_send.at[step],
            recv_sem=sum_recv.at[step],
            device_id=(lax.rem(sp_me + step, sp_count), tp_me),
            device_id_type=MESH,
        )
        copy.start()
        sum_copies.append(copy)

    query_f, query_b = [], []
    for block in range(blocks):
        rows = pl.ds(block * BLK, BLK)
        queries = rotated(q_ref[rows, :], rows) * KEY_CHANNELS ** (-0.5)
        keys = key_ref[rows, :]
        total_f, total_b = cumul_f[block], cumul_b[block]
        middle_f = total_f[BLK // 2 - 1 : BLK // 2]
        middle_b = total_b[BLK // 2 : BLK // 2 + 1]
        scaled_qf = queries * jnp.exp(total_f - middle_f)
        scaled_qb = queries * jnp.exp(total_b - middle_b)
        scaled_kf = (keys * jnp.exp(middle_f - total_f)).astype(jnp.bfloat16)
        scaled_kb = (keys * jnp.exp(middle_b - total_b)).astype(jnp.bfloat16)
        query_f.append((queries * jnp.exp(total_f)).astype(jnp.bfloat16))
        query_b.append((queries * jnp.exp(total_b)).astype(jnp.bfloat16))
        for h in range(heads):
            mine = lane_head == h
            scores_f = dot_nt(jnp.where(mine, scaled_qf, 0.0).astype(jnp.bfloat16), scaled_kf)
            scores_b = dot_nt(jnp.where(mine, scaled_qb, 0.0).astype(jnp.bfloat16), scaled_kb)
            scores = jnp.where(lower, scores_f, 0.0) + jnp.where(upper, scores_b, 0.0)
            within_ref[rows, h * DV : (h + 1) * DV] = jnp.dot(
                scores.astype(jnp.bfloat16),
                v_ref[rows, h * DV : (h + 1) * DV],
                preferred_element_type=jnp.float32,
            )

    for copy in sum_copies:
        copy.wait()
    carry_f = jnp.zeros((DV, lanes), jnp.float32)
    carry_b = jnp.zeros((DV, lanes), jnp.float32)
    for step in range(sp_count - 1, 0, -1):
        state = got_ref[step, 0:DV, :].astype(jnp.float32)
        through = got_ref[step, 2 * DV : 2 * DV + 16, :].astype(jnp.float32)[0:1]
        carry_f = jnp.where(step <= sp_me, carry_f * through + state, carry_f)
    for step in range(1, sp_count):
        state = got_ref[step, DV : 2 * DV, :].astype(jnp.float32)
        through = got_ref[step, 2 * DV : 2 * DV + 16, :].astype(jnp.float32)[8:9]
        carry_b = jnp.where(step > sp_me, carry_b * through + state, carry_b)

    def unpacked(carry):
        return jnp.where(own_head, jnp.concatenate([carry] * heads, axis=0), 0.0)

    state = unpacked(carry_f)
    for block in range(blocks):
        rows = pl.ds(block * BLK, BLK)
        within_ref[rows, :] += dot_nt(query_f[block], state.astype(jnp.bfloat16))
        if block < blocks - 1:
            state = state * decay_f[block] + sums_f[block]
    state = unpacked(carry_b)
    for block in range(blocks - 1, -1, -1):
        rows = pl.ds(block * BLK, BLK)
        attended = within_ref[rows, :] + dot_nt(query_b[block], state.astype(jnp.bfloat16))
        if block > 0:
            state = state * decay_b[block] + sums_b[block]
        for h in range(heads):
            part = attended[:, h * DV : (h + 1) * DV]
            square = jnp.mean(part * part, axis=-1, keepdims=True)
            gate = gate_ref[rows, h * DV : (h + 1) * DV].astype(jnp.float32)
            mixed_ref[rows, h * DV : (h + 1) * DV] = (
                part
                * lax.rsqrt(square + EPS)
                * gain_ref[:, h * DV : (h + 1) * DV]
                * (gate / (1.0 + jnp.exp(-gate)))
            ).astype(jnp.bfloat16)

    row_copies = []
    for step in range(1, tp_count):
        target = lax.rem(tp_me + step, tp_count)
        copy = pltpu.make_async_remote_copy(
            src_ref=mixed_ref.at[pl.ds(pl.multiple_of(target * rows_out, rows_out), rows_out)],
            dst_ref=land_ref.at[tp_me],
            send_sem=row_send.at[step],
            recv_sem=row_recv.at[step],
            device_id=(sp_me, target),
            device_id_type=MESH,
        )
        copy.start()
        row_copies.append(copy)
    land_ref[tp_me] = mixed_ref[pl.ds(pl.multiple_of(tp_me * rows_out, rows_out), rows_out), :]
    for copy in row_copies:
        copy.wait()
    for source in range(tp_count):
        out_ref[:, source * width : (source + 1) * width] = land_ref[source]


def attention(queries, key_rows, values, out_gate, fwd_log, bwd_log, cosine, signed_sine, gain):
    sp_count = lax.axis_size("sp")
    tp_count = lax.axis_size("tp")
    span, lanes = queries.shape
    width = values.shape[1]
    rows_out = span // tp_count
    blocks = span // BLK
    vmem = pl.BlockSpec(memory_space=pltpu.VMEM)
    return pl.pallas_call(
        functools.partial(attention_kernel, sp_count, tp_count),
        out_shape=jax.ShapeDtypeStruct((rows_out, tp_count * width), jnp.bfloat16),
        in_specs=[vmem] * 9,
        out_specs=vmem,
        scratch_shapes=[
            pltpu.VMEM((2 * DV + 16, lanes), jnp.bfloat16),
            pltpu.VMEM((sp_count, 2 * DV + 16, lanes), jnp.bfloat16),
            pltpu.VMEM((span, width), jnp.bfloat16),
            pltpu.VMEM((tp_count, rows_out, width), jnp.bfloat16),
            pltpu.VMEM((span, width), jnp.float32),
            pltpu.VMEM((span, lanes), jnp.float32),
            pltpu.VMEM((blocks, width, lanes), jnp.float32),
            pltpu.VMEM((blocks, width, lanes), jnp.float32),
            pltpu.SemaphoreType.DMA((sp_count,)),
            pltpu.SemaphoreType.DMA((sp_count,)),
            pltpu.SemaphoreType.DMA((tp_count,)),
            pltpu.SemaphoreType.DMA((tp_count,)),
        ],
        compiler_params=pltpu.CompilerParams(collective_id=0, has_side_effects=True),
    )(queries, key_rows, values, out_gate, fwd_log, bwd_log, cosine, signed_sine, gain)


def feed_forward(row_data, gate_parts, up_parts, down_mat):
    groups, _, width = gate_parts.shape
    total = jnp.zeros((row_data.shape[0], down_mat.shape[1]), jnp.float32)
    for group in range(groups):
        hidden = (
            jax.nn.silu(jnp.dot(row_data, gate_parts[group], preferred_element_type=jnp.float32))
            * jnp.dot(row_data, up_parts[group], preferred_element_type=jnp.float32)
        ).astype(jnp.bfloat16)
        total = total + jnp.dot(
            hidden,
            down_mat[group * width : (group + 1) * width],
            preferred_element_type=jnp.float32,
        )
    return total


def slot_map(route_block, experts, capacity):
    tokens, choices = route_block.shape
    flat_ids = route_block.reshape(-1)
    total = flat_ids.shape[0]
    onehot = (flat_ids[:, None] == jnp.arange(experts, dtype=jnp.int32)[None, :]).astype(
        jnp.bfloat16
    )
    earlier = (jnp.arange(total)[:, None] > jnp.arange(total)[None, :]).astype(jnp.bfloat16)
    before = jnp.dot(earlier, onehot, preferred_element_type=jnp.float32)
    slot_ids = jnp.sum(before * onehot.astype(jnp.float32), axis=1).astype(jnp.int32)
    return (flat_ids * capacity + slot_ids).reshape(tokens, choices)


def body(
    stream,
    queries,
    key_rows,
    values,
    out_gate,
    fwd_decay,
    bwd_decay,
    head_gain,
    out_proj,
    mix_gain,
    ffn_gain,
    moe_gain,
    routes,
    route_weight,
    expert_gate,
    expert_up,
    expert_down,
    shared_gate,
    shared_up,
    shared_down,
):
    tokens_here = stream.shape[0]
    span_rows = queries.shape[0]
    experts = lax.axis_size("sp")
    capacity = max(2, 3 * tokens_here * TOPK // (2 * experts))
    gate_parts = lax.all_gather(expert_gate[0], "tp")
    up_parts = lax.all_gather(expert_up[0], "tp")
    down_mat = lax.all_gather(expert_down[0], "tp", axis=0, tiled=True)
    shared_width = shared_gate.shape[1]
    shared_all = lax.all_gather(
        jnp.concatenate([shared_gate, shared_up, shared_down.T], axis=1), "tp"
    )
    rows_of = slot_map(routes, experts, capacity)
    slots = jnp.arange(experts * capacity, dtype=jnp.int32)
    taken = rows_of[:, :, None] == slots[None, None, :]
    pick = jnp.any(taken, axis=1).astype(jnp.bfloat16)
    weights = jnp.sum(jnp.where(taken, route_weight[:, :, None], 0.0), axis=1)
    weights_high = weights.astype(jnp.bfloat16)
    weights_low = (weights - weights_high.astype(jnp.float32)).astype(jnp.bfloat16)
    offset = lax.axis_index("sp") * span_rows
    positions = (offset + jnp.arange(span_rows, dtype=jnp.int32)).astype(jnp.float32)
    lanes = queries.shape[1]
    half = KEY_CHANNELS // 2
    lane = jnp.arange(lanes, dtype=jnp.int32) % KEY_CHANNELS
    frequency = ROPE_BASE ** (-(lane % half).astype(jnp.float32) / half)
    angles = positions[:, None] * frequency[None, :]
    sine = jnp.sin(angles)
    mixed_out = attention(
        queries,
        key_rows,
        values,
        out_gate,
        jax.nn.log_sigmoid(fwd_decay) / GATE_NORM,
        jax.nn.log_sigmoid(bwd_decay) / GATE_NORM,
        jnp.cos(angles),
        jnp.where(lane[None, :] < half, -sine, sine),
        head_gain.reshape(1, -1),
    )
    projected = jnp.dot(mixed_out, out_proj, preferred_element_type=jnp.float32)
    residual = (stream.astype(jnp.float32) + normalize(projected) * mix_gain).astype(jnp.bfloat16)
    normed = (normalize(residual.astype(jnp.float32)) * ffn_gain).astype(jnp.bfloat16)
    model_width = normed.shape[1]
    outgoing = lax.dot_general(
        pick, normed, (((0,), (0,)), ((), ())), preferred_element_type=jnp.float32
    ).astype(jnp.bfloat16)
    arrived = lax.all_to_all(
        outgoing.reshape(experts, capacity, model_width),
        "sp",
        split_axis=0,
        concat_axis=0,
        tiled=True,
    )
    shared_sum = jnp.zeros((tokens_here, model_width), jnp.float32)
    for group in range(lax.axis_size("tp")):
        both = jnp.dot(
            normed, shared_all[group, :, : 2 * shared_width], preferred_element_type=jnp.float32
        )
        hidden = (jax.nn.silu(both[:, :shared_width]) * both[:, shared_width:]).astype(
            jnp.bfloat16
        )
        shared_sum = shared_sum + dot_nt(hidden, shared_all[group, :, 2 * shared_width :])
    routed_done = feed_forward(
        arrived.reshape(experts * capacity, model_width), gate_parts, up_parts, down_mat
    ).astype(jnp.bfloat16)
    routed_back = lax.all_to_all(
        routed_done.reshape(experts, capacity, model_width),
        "sp",
        split_axis=0,
        concat_axis=0,
        tiled=True,
    ).reshape(experts * capacity, model_width)
    mixture = (
        shared_sum
        + jnp.dot(weights_high, routed_back, preferred_element_type=jnp.float32)
        + jnp.dot(weights_low, routed_back, preferred_element_type=jnp.float32)
    )
    return (residual.astype(jnp.float32) + normalize(mixture) * moe_gain).astype(jnp.bfloat16)


def solution(mesh):
    return jax.shard_map(
        body,
        mesh=mesh,
        in_specs=(
            P(("sp", "tp"), None),
            P("sp", "tp"),
            P("sp", "tp"),
            P("sp", "tp"),
            P("sp", "tp"),
            P("sp", "tp"),
            P("sp", "tp"),
            P("tp"),
            P(),
            P(),
            P(),
            P(),
            P(("sp", "tp"), None),
            P(("sp", "tp"), None),
            P("sp", None, "tp"),
            P("sp", None, "tp"),
            P("sp", "tp", None),
            P(None, "tp"),
            P(None, "tp"),
            P("tp", None),
        ),
        out_specs=P(("sp", "tp"), None),
        check_vma=False,
    )
```

time: 288 us -> 196 us (0.68)
  matrix products: 83 us -> 38.7 us
  local copies, waits for them, and re-layouts: 42.4 us -> 10.1 us
  other arithmetic: 32.2 us -> 6 us
  Pallas kernels: 0 us -> 25.1 us
  waiting for transfers between devices: 66.7 us -> 51.4 us
  blocking collectives: 33.1 us -> 44.8 us
  starting transfers between devices: 13.4 us -> 5.65 us
    all_to_all x0 -> x1, blocking collectives: none -> 44.8 us  [body(): lax.all_to_all(outgoing.reshape(experts, capacity, model_width), 'sp', sp...]
    all_to_all x2 -> x0, waiting for transfers between devices: 40.7 us -> none  [the longest x1 36.1 us: body(): lax.all_to_all(outgoing.reshape(experts, capacity, model_width), 'sp', sp...]
    all_gather x1 -> x0, blocking collectives: 33.1 us -> none  [carried_in(): gathered = lax.all_gather(packed, axis).astype(jnp.float32)]
    dot_general x36 -> x8, matrix products: 35.5 us -> 6.61 us  [the longest x4 3.98 us: body(): jnp.dot(normed, shared_all[group, :, :2 * shared_width], preferred_elemen...]
    all_gather x1, waiting for transfers between devices: 0.02 us -> 27.4 us  [body(): up_parts = lax.all_gather(expert_up[0], 'tp')]
    pallas_call x0 -> x1, Pallas kernels: none -> 25.1 us  [attention(): pl.pallas_call(functools.partial(attention_kernel, sp_count, tp_count), o...]
    another operation x12 -> x0, other arithmetic: 22.2 us -> none  [the longest x2 14.1 us: blockwise(): jnp.cumsum(log_decay.reshape(block_count, BLK, head_count, key_width), ax...]
    all_to_all x1, waiting for transfers between devices: 22.5 us -> 2.5 us  [body(): lax.all_to_all(routed_done.reshape(experts, capacity, model_width), 'sp',...]
  transfers between devices with their start and end apart: 9 -> 5, of which waited for: 3 -> 3; matrix products, arithmetic and copies ran while one was open for 54% -> 27% of each run, Pallas kernels for 0% -> 13%
where the time goes in v2:
time: 196 us; the launch traced here: 195 us
  waiting for transfers between devices  51.4 us (26%)
  blocking collectives  44.8 us (23%)
  matrix products  38.7 us (20%)
  Pallas kernels  25.1 us (13%)
  between operations  13.5 us (7%)
  local copies, waits for them, and re-layouts  10.1 us (5%)
  other arithmetic  6 us (3%)
  starting transfers between devices  5.65 us (3%)
    all_to_all x1, blocking collectives, body(): lax.all_to_all(outgoing.reshape(experts, capacity, model_width), 'sp', sp...  44.8 us
    all_gather x1, waiting for transfers between devices, body(): up_parts = lax.all_gather(expert_up[0], 'tp')  27.4 us
    pallas_call x1, Pallas kernels, attention(): pl.pallas_call(functools.partial(attention_kernel, sp_count, tp_count), o...  25.1 us
    dot_general x4, matrix products, feed_forward(): jnp.dot(hidden, down_mat[group * width:(group + 1) * width], preferred_el...  22.7 us
    all_gather x1, waiting for transfers between devices, body(): lax.all_gather(jnp.concatenate([shared_gate, shared_up, shared_down.T], a...  19.4 us
    all_gather x1, local copies, waits for them, and re-layouts, body(): lax.all_gather(jnp.concatenate([shared_gate, shared_up, shared_down.T], a...  8.65 us
    all_to_all x1, starting transfers between devices, body(): lax.all_to_all(routed_done.reshape(experts, capacity, model_width), 'sp',...  5.53 us
    dot_general x4, matrix products, feed_forward(): jnp.dot(row_data, gate_parts[group], preferred_element_type=jnp.float32)  4.42 us
  transfers between devices with their start and end apart: 5, of which 3 were waited for; matrix products, arithmetic and copies ran while one was open for 27% of the time, Pallas kernels for 13%

profile of v2, /device:TPU:0, one launch (start us, length us, event | category | flops | bytes accessed | tf_op | source)
XLA Modules:
  0.0 195.3 jit_solution(7423258004251834353)
XLA Ops:
  6.5 0.0 all-gather.7.cloned.1.call-start
  6.5 0.7 all-gather.7.cloned.1.call-update
  7.3 0.0 all-gather.13.cloned.1.call-start
  7.3 0.7 all-gather.13.cloned.1.call-update
  8.0 0.0 all-gather.9.cloned.1.call-start
  8.1 0.7 all-gather.9.cloned.1.call-update
  8.7 0.0 all-gather.11.cloned.1.call-start
  8.8 0.0 copy-done.1
  8.8 0.2 copy.46
  9.0 0.0 copy-done.2
  9.0 0.0 copy-start.11
  9.0 0.0 copy-start.6
  9.1 0.0 copy-start.7
  9.1 0.2 copy.47
  9.3 0.0 copy-done.3
  9.3 1.4 pad_maximum_fusion
  10.6 0.0 all-gather.11.cloned.1.call-update
  10.7 0.0 copy-done.11
  10.7 0.1 copy.49
  10.8 0.1 eq.31
  10.9 0.2 fusion.7
  11.2 0.1 convert_element_type.98
  11.3 0.1 copy.50
  11.4 1.8 negate_select_fusion
  13.3 0.0 copy-done.6
  13.3 0.0 copy-done.7
  13.3 1.1 fusion.43
  14.4 25.1 %shard_map.190 = bf16[128,1024]{1,0:T(8,128)(2,1)} custom-call(bf16[512,128]{1,0:T(8,128)(2,1)} %q_ref.1, bf16[512,128]{1,0:T(8,128)(2,1)} %k_ref.1, bf16[512,256]{1,0:T(8,128)(2,1)} %v_ref.1, bf16[512,256]{1,0:T(8,128)(2,1)} %gate_ref.1, f32[512,128]{1,0:T(8,128)} %get-tuple-element.13.fwd_ref, f32[512,128]{1,0:T(8,128)} %get-tuple-element.14.bwd_ref, ...), custom_call_target="tpu_custom_call" | custom-call | tf_op jit(solution)/shard_map/pallas_call | solution.py:259
  39.5 0.0 copy-start.4
  39.5 0.0 copy-start.8
  39.5 0.1 fusion.41
  39.7 0.0 copy-start.9
  39.7 3.1 %multiply_reduce_fusion.1 = (f32[128]{0:T(128)S(1)}, f32[128,2048]{1,0:T(8,128)S(1)}) fusion(bf16[128,1024]{1,0:T(8,128)(2,1)} %shard_map.190, bf16[1024,2048]{1,0:T(8,128)(2,1)} %param.28), kind=kOutput, calls=%fused_computation.54 | convolution fusion | flops 537395072 | bytes 5505536 | tf_op jit(solution)/shard_map/dot_general | solution.py:370
  42.8 0.0 copy-done.4
  42.8 0.4 fusion.8
  43.2 0.7 convolution_convert_fusion
  43.9 44.8 %all_to_all.10 = bf16[8,48,2048]{2,1,0:T(8,128)(2,1)S(1)} all-to-all(bf16[8,48,2048]{2,1,0:T(8,128)(2,1)S(1)} %bitcast.103), channel_id=1, replica_groups=mesh['sp'=8,'tp'=4] {'sp'}, dimensions={0} | all-to-all | bytes 3145728 | tf_op jit(solution)/shard_map/all_to_all | solution.py:377
  88.7 1.9 fusion.13
  90.7 0.5 copy-done.13
  91.2 0.6 fusion.14
  91.8 0.6 fusion.15
  92.4 1.3 fusion.12
  93.7 27.4 %all-gather.9.cloned.1.call-done = bf16[4,2048,256]{2,1,0:T(8,128)(2,1)} async-done(((bf16[1,2048,256]{2,1,0:T(8,128)(2,1)}), bf16[4,2048,256]{2,1,0:T(8,128)(2,1)}) %all-gather.9.cloned.1.call-update) | async-done | bytes 4194320 | tf_op jit(solution)/shard_map/all_gather | solution.py:338
  121.1 5.0 %fusion.4 = f32[384,2048]{1,0:T(8,128)} fusion(bf16[384,2048]{1,0:T(8,128)(2,1)S(1)} %bitcast.89, bf16[1,1024,2048]{2,1,0:T(8,128)(2,1)} %all-gather.13.cloned.1.call-done, bf16[4,2048,256]{2,1,0:T(8,128)(2,1)} %all-gather.9.cloned.1.call-done, f32[384,256]{1,0:T(8,128)S(1)} %fusion.13), kind=kOutput, calls=%fused_computation.19 | convolution fusion | flops 805896192 | bytes 7208960 | tf_op jit(solution)/shard_map/dot_general | solution.py:290
  126.1 5.0 %fusion.5 = f32[384,2048]{1,0:T(8,128)} fusion(bf16[384,2048]{1,0:T(8,128)(2,1)S(1)} %bitcast.90, bf16[1,1024,2048]{2,1,0:T(8,128)(2,1)} %all-gather.13.cloned.1.call-done, bf16[4,2048,256]{2,1,0:T(8,128)(2,1)} %all-gather.9.cloned.1.call-done, f32[384,256]{1,0:T(8,128)S(1)} %fusion.14), kind=kOutput, calls=%fused_computation.20 | convolution fusion | flops 805896192 | bytes 7208960 | tf_op jit(solution)/shard_map/dot_general | solution.py:290
  131.1 5.3 %fusion.6 = f32[384,2048]{1,0:T(8,128)} fusion(bf16[384,2048]{1,0:T(8,128)(2,1)S(1)} %bitcast.91, bf16[1,1024,2048]{2,1,0:T(8,128)(2,1)} %all-gather.13.cloned.1.call-done, bf16[4,2048,256]{2,1,0:T(8,128)(2,1)} %all-gather.9.cloned.1.call-done, f32[384,256]{1,0:T(8,128)S(1)} %fusion.15), kind=kOutput, calls=%fused_computation.21 | convolution fusion | flops 805896192 | bytes 7208960 | tf_op jit(solution)/shard_map/dot_general | solution.py:290
  136.4 0.0 copy-done.5
  136.4 7.4 %add_convert_fusion = bf16[384,2048]{1,0:T(8,128)(2,1)} fusion(f32[384,2048]{1,0:T(8,128)} %fusion.4, f32[384,2048]{1,0:T(8,128)} %fusion.6, f32[384,2048]{1,0:T(8,128)} %fusion.5, bf16[1,1024,2048]{2,1,0:T(8,128)(2,1)} %all-gather.13.cloned.1.call-done, bf16[384,2048]{1,0:T(8,128)(2,1)S(1)} %bitcast.92, ...), kind=kOutput, calls=%fused_computation | convolution fusion | flops 809041920 | bytes 15073280 | tf_op jit(solution)/shard_map/dot_general | solution.py:290
  143.8 5.5 %all-to-all-start.1 = ((bf16[8,48,2048]{2,1,0:T(8,128)(2,1)}), bf16[8,48,2048]{2,1,0:T(8,128)(2,1)S(1)}, u32[]{:S(2)}, u32[]{:S(2)}) async-start(bf16[8,48,2048]{2,1,0:T(8,128)(2,1)} %bitcast.25), calls=%async_computation.1 | async-start | bytes 3145728 | tf_op jit(solution)/shard_map/all_to_all | solution.py:396
  149.3 0.1 select_reduce_fusion
  149.5 19.4 %all-gather.11.cloned.1.call-done = bf16[8192,384]{0,1:T(8,128)(2,1)} async-done(((bf16[2048,384]{0,1:T(8,128)(2,1)}), bf16[8192,384]{0,1:T(8,128)(2,1)}) %all-gather.11.cloned.1.call-update) | async-done | bytes 6291472 | tf_op jit(solution)/shard_map/all_gather | solution.py:341
  168.9 8.6 %copy.48 = bf16[8192,384]{1,0:T(8,128)(2,1)} copy(bf16[8192,384]{0,1:T(8,128)(2,1)} %all-gather.11.cloned.1.call-done) | data formatting | bytes 12582912 | tf_op jit(solution)/shard_map/all_gather | solution.py:341
  177.5 1.7 fusion.19
  179.3 1.7 fusion.20
  181.0 1.6 fusion.18
  182.6 0.3 fusion.17
  182.9 0.3 fusion.16
  183.3 0.3 convolution_add_fusion.4
  183.6 0.3 convolution_add_fusion.3
  183.9 0.3 convolution_add_fusion.2
  184.2 2.5 %all-to-all-done.1 = bf16[8,48,2048]{2,1,0:T(8,128)(2,1)S(1)} async-done(((bf16[8,48,2048]{2,1,0:T(8,128)(2,1)}), bf16[8,48,2048]{2,1,0:T(8,128)(2,1)S(1)}, u32[]{:S(2)}, u32[]{:S(2)}) %all-to-all-start.1) | async-done | bytes 1572896 | tf_op jit(solution)/shard_map/all_to_all | solution.py:396
  186.7 0.4 convolution_add_fusion.1
  187.2 0.5 multiply_reduce_fusion
  187.7 1.0 fusion.11
  (23 shorter events, 0.1 us)
Async XLA Ops:
  6.5 2.3 %copy-start.1 = (bf16[2048,128]{1,0:T(8,128)(2,1)S(1)}, bf16[2048,128]{1,0:T(8,128)(2,1)}, u32[]{:S(2)}) copy-start(bf16[2048,128]{1,0:T(8,128)(2,1)} %param.37) | copy-start | bytes 1572868
  6.5 2.5 %copy-start.2 = (bf16[2048,128]{1,0:T(8,128)(2,1)S(1)}, bf16[2048,128]{1,0:T(8,128)(2,1)}, u32[]{:S(2)}) copy-start(bf16[2048,128]{1,0:T(8,128)(2,1)} %param.38) | copy-start | bytes 1572868
  6.5 2.8 %copy-start.3 = (bf16[128,2048]{1,0:T(8,128)(2,1)S(1)}, bf16[128,2048]{1,0:T(8,128)(2,1)}, u32[]{:S(2)}) copy-start(bf16[128,2048]{1,0:T(8,128)(2,1)} %param.39) | copy-start | bytes 1572868
  6.5 82.2 %all-gather.7.cloned.1.call-start = ((), (), s32[]{:S(2)}) async-start(), calls=%async_computation.2 | async-start | bytes 5242880 | tf_op jit(solution)/shard_map/all_gather | solution.py:337
  7.3 86.4 %all-gather.13.cloned.1.call-start = ((), (), s32[]{:S(2)}) async-start(), calls=%async_computation.5 | async-start | bytes 5242880 | tf_op jit(solution)/shard_map/all_gather | solution.py:339
  8.0 113.1 %all-gather.9.cloned.1.call-start = ((), (), s32[]{:S(2)}) async-start(), calls=%async_computation.3 | async-start | bytes 5242880 | tf_op jit(solution)/shard_map/all_gather | solution.py:338
  8.7 160.2 %all-gather.11.cloned.1.call-start = ((), (), s32[]{:S(2)}) async-start(), calls=%async_computation.4 | async-start | bytes 7864320 | tf_op jit(solution)/shard_map/all_gather | solution.py:341
  9.0 1.6 copy-start.11
  9.0 4.2 %copy-start.6 = (f32[512,128]{1,0:T(8,128)S(1)}, f32[512,128]{1,0:T(8,128)}, u32[]{:S(2)}) copy-start(f32[512,128]{1,0:T(8,128)} %param.25) | copy-start | bytes 786436
  9.1 4.2 %copy-start.7 = (f32[512,128]{1,0:T(8,128)S(1)}, f32[512,128]{1,0:T(8,128)}, u32[]{:S(2)}) copy-start(f32[512,128]{1,0:T(8,128)} %param.26) | copy-start | bytes 786436
  39.5 3.3 %copy-start.4 = (bf16[128,2048]{1,0:T(8,128)(2,1)S(1)}, bf16[128,2048]{1,0:T(8,128)(2,1)}, u32[]{:S(2)}) copy-start(bf16[128,2048]{1,0:T(8,128)(2,1)} %param.20) | copy-start | bytes 1572868
  39.5 3.3 %copy-start.8 = (f32[2048]{0:T(1024)S(1)}, f32[2048]{0:T(1024)}, u32[]{:S(2)}) copy-start(f32[2048]{0:T(1024)} %param.29) | copy-start | bytes 24580
  39.7 3.5 %copy-start.9 = (f32[2048]{0:T(1024)S(1)}, f32[2048]{0:T(1024)}, u32[]{:S(2)}) copy-start(f32[2048]{0:T(1024)} %param.30) | copy-start | bytes 24580
  88.7 2.5 %copy-start.13 = (bf16[4,2048,256]{2,1,0:T(8,128)(2,1)S(1)}, bf16[4,2048,256]{2,1,0:T(8,128)(2,1)}, u32[]{:S(2)}) copy-start(bf16[4,2048,256]{2,1,0:T(8,128)(2,1)} %all-gather.7.cloned.1.call-done) | copy-start | bytes 12582916
  131.1 5.3 %copy-start.5 = (f32[384,256]{1,0:T(8,128)S(1)}, f32[384,256]{1,0:T(8,128)}, u32[]{:S(2)}) copy-start(f32[384,256]{1,0:T(8,128)} %fusion.12) | copy-start | bytes 1179652
  143.8 5.5 %copy-start.12 = (f32[128,2]{0,1:T(2,128)S(1)}, f32[128,2]{0,1:T(2,128)}, u32[]{:S(2)}) copy-start(f32[128,2]{0,1:T(2,128)} %param.33) | copy-start | bytes 3076
  143.8 42.9 %all-to-all-start.1 = ((bf16[8,48,2048]{2,1,0:T(8,128)(2,1)}), bf16[8,48,2048]{2,1,0:T(8,128)(2,1)S(1)}, u32[]{:S(2)}, u32[]{:S(2)}) async-start(bf16[8,48,2048]{2,1,0:T(8,128)(2,1)} %bitcast.25), calls=%async_computation.1 | async-start | bytes 3145728 | tf_op jit(solution)/shard_map/all_to_all | solution.py:396
  177.5 5.0 %copy-start = (bf16[8192,384]{1,0:T(8,128)(2,1)S(1)}, bf16[8192,384]{1,0:T(8,128)(2,1)}, u32[]{:S(2)}) copy-start(bf16[8192,384]{1,0:T(8,128)(2,1)} %copy.48) | copy-start | bytes 18874372
  186.7 1.0 copy-start.10
Sparse Core Ops, SparseCore 0:
  8.9 39.9 all-gather.6
  50.5 34.5 all-gather.12
  86.6 34.4 all-gather.8
  122.5 46.3 all-gather.10

commit v3 on v2

--- a/solution.py
+++ b/solution.py
@@ -279,20 +279,253 @@
     )(queries, key_rows, values, out_gate, fwd_log, bwd_log, cosine, signed_sine, gain)
 
 
-def feed_forward(row_data, gate_parts, up_parts, down_mat):
-    groups, _, width = gate_parts.shape
-    total = jnp.zeros((row_data.shape[0], down_mat.shape[1]), jnp.float32)
+def dispatch_kernel(
+    sp_count,
+    tp_count,
+    outgoing_ref,
+    rows_ref,
+    gate_ref,
+    up_ref,
+    down_ref,
+    arrived_ref,
+    shared_ref,
+    block_land,
+    row_land,
+    part_ref,
+    part_land,
+    block_send,
+    block_recv,
+    row_send,
+    row_recv,
+    part_send,
+    part_recv,
+):
+    sp_me = lax.axis_index("sp")
+    tp_me = lax.axis_index("tp")
+
+    def sp_peer(step):
+        return (lax.rem(sp_me + step, sp_count), tp_me)
+
+    def tp_peer(step):
+        return (sp_me, lax.rem(tp_me + step, tp_count))
+
+    barrier = pltpu.get_barrier_semaphore()
+    for step in range(1, sp_count):
+        pl.semaphore_signal(barrier, inc=1, device_id=sp_peer(step), device_id_type=MESH)
+    for step in range(1, tp_count):
+        pl.semaphore_signal(barrier, inc=1, device_id=tp_peer(step), device_id_type=MESH)
+    pl.semaphore_wait(barrier, sp_count - 1 + tp_count - 1)
+
+    row_copies, block_copies, part_copies = [], [], []
+    for step in range(1, tp_count):
+        copy = pltpu.make_async_remote_copy(
+            src_ref=rows_ref,
+            dst_ref=row_land.at[step],
+            send_sem=row_send.at[step],
+            recv_sem=row_recv.at[step],
+            device_id=tp_peer(step),
+            device_id_type=MESH,
+        )
+        copy.start()
+        row_copies.append(copy)
+    for step in range(1, sp_count):
+        copy = pltpu.make_async_remote_copy(
+            src_ref=outgoing_ref.at[lax.rem(sp_me + step, sp_count)],
+            dst_ref=block_land.at[sp_me],
+            send_sem=block_send.at[step],
+            recv_sem=block_recv.at[step],
+            device_id=sp_peer(step),
+            device_id_type=MESH,
+        )
+        copy.start()
+        block_copies.append(copy)
+    block_land[sp_me] = outgoing_ref[sp_me]
+
+    def partial(rows):
+        hidden = jax.nn.silu(
+            jnp.dot(rows, gate_ref[...], preferred_element_type=jnp.float32)
+        ) * jnp.dot(rows, up_ref[...], preferred_element_type=jnp.float32)
+        return jnp.dot(
+            hidden.astype(jnp.bfloat16), down_ref[...], preferred_element_type=jnp.float32
+        )
+
+    shared_ref[...] = partial(rows_ref[...])
+    for step in range(1, tp_count):
+        row_copies[step - 1].wait()
+        part_ref[step] = partial(row_land[step]).astype(jnp.bfloat16)
+        copy = pltpu.make_async_remote_copy(
+            src_ref=part_ref.at[step],
+            dst_ref=part_land.at[step],
+            send_sem=part_send.at[step],
+            recv_sem=part_recv.at[step],
+            device_id=tp_peer(tp_count - step),
+            device_id_type=MESH,
+        )
+        copy.start()
+        part_copies.append(copy)
+    for step in range(1, tp_count):
+        part_copies[step - 1].wait()
+        shared_ref[...] += part_land[step].astype(jnp.float32)
+    for copy in block_copies:
+        copy.wait()
+    arrived_ref[...] = block_land[...]
+
+
+def dispatch(outgoing, normed, shared_gate, shared_up, shared_down):
+    sp_count = lax.axis_size("sp")
+    tp_count = lax.axis_size("tp")
+    vmem = pl.BlockSpec(memory_space=pltpu.VMEM)
+    several = pltpu.VMEM((tp_count,) + normed.shape, normed.dtype)
+    return pl.pallas_call(
+        functools.partial(dispatch_kernel, sp_count, tp_count),
+        out_shape=(
+            jax.ShapeDtypeStruct(outgoing.shape, outgoing.dtype),
+            jax.ShapeDtypeStruct(normed.shape, jnp.float32),
+        ),
+        in_specs=[vmem] * 5,
+        out_specs=(vmem, vmem),
+        scratch_shapes=[
+            pltpu.VMEM(outgoing.shape, outgoing.dtype),
+            several,
+            several,
+            several,
+            pltpu.SemaphoreType.DMA((sp_count,)),
+            pltpu.SemaphoreType.DMA((sp_count,)),
+            pltpu.SemaphoreType.DMA((tp_count,)),
+            pltpu.SemaphoreType.DMA((tp_count,)),
+            pltpu.SemaphoreType.DMA((tp_count,)),
+            pltpu.SemaphoreType.DMA((tp_count,)),
+        ],
+        compiler_params=pltpu.CompilerParams(collective_id=1, has_side_effects=True),
+    )(outgoing, normed, shared_gate, shared_up, shared_down)
+
+
+def expert_kernel(
+    sp_count,
+    rows_ref,
+    gate_hbm,
+    up_hbm,
+    down_hbm,
+    high_ref,
+    low_ref,
+    shared_ref,
+    residual_ref,
+    gain_ref,
+    out_ref,
+    gate_ref,
+    up_ref,
+    down_ref,
+    total_ref,
+    done_ref,
+    back_ref,
+    weight_sem,
+    send_sem,
+    recv_sem,
+):
+    sp_me = lax.axis_index("sp")
+    tp_me = lax.axis_index("tp")
+    groups, _, width = gate_ref.shape
+    capacity = done_ref.shape[1]
+
+    fetches = []
     for group in range(groups):
+        cut = pl.ds(group * width, width)
+        trio = (
+            pltpu.make_async_copy(gate_hbm.at[group], gate_ref.at[group], weight_sem.at[0, group]),
+            pltpu.make_async_copy(up_hbm.at[group], up_ref.at[group], weight_sem.at[1, group]),
+            pltpu.make_async_copy(down_hbm.at[cut], down_ref.at[cut], weight_sem.at[2, group]),
+        )
+        for copy in trio:
+            copy.start()
+        fetches.append(trio)
+
+    barrier = pltpu.get_barrier_semaphore()
+    for step in range(1, sp_count):
+        pl.semaphore_signal(
+            barrier,
+            inc=1,
+            device_id=(lax.rem(sp_me + step, sp_count), tp_me),
+            device_id_type=MESH,
+        )
+
+    for group in range(groups):
+        for copy in fetches[group]:
+            copy.wait()
         hidden = (
-            jax.nn.silu(jnp.dot(row_data, gate_parts[group], preferred_element_type=jnp.float32))
-            * jnp.dot(row_data, up_parts[group], preferred_element_type=jnp.float32)
+            jax.nn.silu(jnp.dot(rows_ref[...], gate_ref[group], preferred_element_type=jnp.float32))
+            * jnp.dot(rows_ref[...], up_ref[group], preferred_element_type=jnp.float32)
         ).astype(jnp.bfloat16)
-        total = total + jnp.dot(
+        piece = jnp.dot(
             hidden,
-            down_mat[group * width : (group + 1) * width],
+            down_ref[group * width : (group + 1) * width, :],
             preferred_element_type=jnp.float32,
         )
-    return total
+        if group == 0:
+            total_ref[...] = piece
+        else:
+            total_ref[...] += piece
+    for source in range(sp_count):
+        done_ref[source] = total_ref[source * capacity : (source + 1) * capacity, :].astype(
+            done_ref.dtype
+        )
+
+    pl.semaphore_wait(barrier, sp_count - 1)
+    copies = []
+    for step in range(1, sp_count):
+        target = lax.rem(sp_me + step, sp_count)
+        copy = pltpu.make_async_remote_copy(
+            src_ref=done_ref.at[target],
+            dst_ref=back_ref.at[sp_me],
+            send_sem=send_sem.at[step],
+            recv_sem=recv_sem.at[step],
+            device_id=(target, tp_me),
+            device_id_type=MESH,
+        )
+        copy.start()
+        copies.append(copy)
+    back_ref[sp_me] = done_ref[sp_me]
+    for copy in copies:
+        copy.wait()
+
+    mixture = shared_ref[...]
+    for expert in range(sp_count):
+        mixture = mixture + jnp.dot(
+            high_ref[expert], back_ref[expert], preferred_element_type=jnp.float32
+        )
+        mixture = mixture + jnp.dot(
+            low_ref[expert], back_ref[expert], preferred_element_type=jnp.float32
+        )
+    square = jnp.mean(mixture * mixture, axis=-1, keepdims=True)
+    out_ref[...] = (
+        residual_ref[...].astype(jnp.float32)
+        + mixture * lax.rsqrt(square + EPS) * gain_ref[...]
+    ).astype(out_ref.dtype)
+
+
+def run_expert(rows, gate_parts, up_parts, down_mat, high, low, shared_sum, residual, gain):
+    sp_count = lax.axis_size("sp")
+    groups = gate_parts.shape[0]
+    vmem = pl.BlockSpec(memory_space=pltpu.VMEM)
+    hbm = pl.BlockSpec(memory_space=pl.ANY)
+    blocked = pltpu.VMEM((sp_count, rows.shape[0] // sp_count, rows.shape[1]), rows.dtype)
+    return pl.pallas_call(
+        functools.partial(expert_kernel, sp_count),
+        out_shape=jax.ShapeDtypeStruct(residual.shape, residual.dtype),
+        in_specs=[vmem, hbm, hbm, hbm] + [vmem] * 5,
+        out_specs=vmem,
+        scratch_shapes=[
+            pltpu.VMEM(gate_parts.shape, gate_parts.dtype),
+            pltpu.VMEM(up_parts.shape, up_parts.dtype),
+            pltpu.VMEM(down_mat.shape, down_mat.dtype),
+            pltpu.VMEM(rows.shape, jnp.float32),
+            blocked,
+            blocked,
+            pltpu.SemaphoreType.DMA((3, groups)),
+            pltpu.SemaphoreType.DMA((sp_count,)),
+            pltpu.SemaphoreType.DMA((sp_count,)),
+        ],
+        compiler_params=pltpu.CompilerParams(collective_id=2, has_side_effects=True),
+    )(rows, gate_parts, up_parts, down_mat, high, low, shared_sum, residual, gain)
 
 
 def slot_map(route_block, experts, capacity):
@@ -337,15 +570,12 @@
     gate_parts = lax.all_gather(expert_gate[0], "tp")
     up_parts = lax.all_gather(expert_up[0], "tp")
     down_mat = lax.all_gather(expert_down[0], "tp", axis=0, tiled=True)
-    shared_width = shared_gate.shape[1]
-    shared_all = lax.all_gather(
-        jnp.concatenate([shared_gate, shared_up, shared_down.T], axis=1), "tp"
-    )
     rows_of = slot_map(routes, experts, capacity)
     slots = jnp.arange(experts * capacity, dtype=jnp.int32)
     taken = rows_of[:, :, None] == slots[None, None, :]
     pick = jnp.any(taken, axis=1).astype(jnp.bfloat16)
     weights = jnp.sum(jnp.where(taken, route_weight[:, :, None], 0.0), axis=1)
+    weights = weights.reshape(tokens_here, experts, capacity).transpose(1, 0, 2)
     weights_high = weights.astype(jnp.bfloat16)
     weights_low = (weights - weights_high.astype(jnp.float32)).astype(jnp.bfloat16)
     offset = lax.axis_index("sp") * span_rows
@@ -374,38 +604,24 @@
     outgoing = lax.dot_general(
         pick, normed, (((0,), (0,)), ((), ())), preferred_element_type=jnp.float32
     ).astype(jnp.bfloat16)
-    arrived = lax.all_to_all(
+    arrived, shared_sum = dispatch(
         outgoing.reshape(experts, capacity, model_width),
-        "sp",
-        split_axis=0,
-        concat_axis=0,
-        tiled=True,
-    )
-    shared_sum = jnp.zeros((tokens_here, model_width), jnp.float32)
-    for group in range(lax.axis_size("tp")):
-        both = jnp.dot(
-            normed, shared_all[group, :, : 2 * shared_width], preferred_element_type=jnp.float32
-        )
-        hidden = (jax.nn.silu(both[:, :shared_width]) * both[:, shared_width:]).astype(
-            jnp.bfloat16
-        )
-        shared_sum = shared_sum + dot_nt(hidden, shared_all[group, :, 2 * shared_width :])
-    routed_done = feed_forward(
-        arrived.reshape(experts * capacity, model_width), gate_parts, up_parts, down_mat
-    ).astype(jnp.bfloat16)
-    routed_back = lax.all_to_all(
-        routed_done.reshape(experts, capacity, model_width),
-        "sp",
-        split_axis=0,
-        concat_axis=0,
-        tiled=True,
-    ).reshape(experts * capacity, model_width)
-    mixture = (
-        shared_sum
-        + jnp.dot(weights_high, routed_back, preferred_element_type=jnp.float32)
-        + jnp.dot(weights_low, routed_back, preferred_element_type=jnp.float32)
-    )
-    return (residual.astype(jnp.float32) + normalize(mixture) * moe_gain).astype(jnp.bfloat16)
+        normed,
+        shared_gate,
+        shared_up,
+        shared_down,
+    )
+    return run_expert(
+        arrived.reshape(experts * capacity, model_width),
+        gate_parts,
+        up_parts,
+        down_mat,
+        weights_high,
+        weights_low,
+        shared_sum,
+        residual,
+        moe_gain.reshape(1, -1),
+    )
 
 
 def solution(mesh):

time: 196 us -> 203 us (1.036)
  the two profiles are of different devices: /device:TPU:0 before, /device:TPU:10 now
where the time goes in v3:
time: 203 us
  Pallas kernels  157 us (77%)
  waiting for transfers between devices  17.9 us (9%)
  between operations  13.3 us (7%)
  other arithmetic  6.11 us (3%)
  matrix products  5.06 us (2%)
  local copies, waits for them, and re-layouts  3.35 us (2%)
    pallas_call x1, Pallas kernels, dispatch(): pl.pallas_call(functools.partial(dispatch_kernel, sp_count, tp_count), ou...  82.1 us
    pallas_call x1, Pallas kernels, run_expert(): pl.pallas_call(functools.partial(expert_kernel, sp_count), out_shape=jax....  49.3 us
    pallas_call x1, Pallas kernels, attention(): pl.pallas_call(functools.partial(attention_kernel, sp_count, tp_count), o...  25.9 us
    all_gather x1, waiting for transfers between devices, body(): down_mat = lax.all_gather(expert_down[0], 'tp', axis=0, tiled=True)  15.8 us
  transfers between devices with their start and end apart: 3, of which 1 were waited for; matrix products, arithmetic and copies ran while one was open for 6% of the time, Pallas kernels for 53%

profile of v3, /device:TPU:10, one launch (start us, length us, event | category | flops | bytes accessed | tf_op | source)
XLA Modules:
  0.0 203.1 jit_solution(9657031078016805356)
XLA Ops:
  6.5 0.0 copy-start.3
  6.5 0.0 copy-start.4
  6.5 0.0 all-gather.5.cloned.1.call-start
  6.5 0.7 all-gather.5.cloned.1.call-update
  7.3 0.0 all-gather.7.cloned.1.call-start
  7.3 0.7 all-gather.7.cloned.1.call-update
  8.0 0.0 all-gather.9.cloned.1.call-start
  8.1 0.7 all-gather.9.cloned.1.call-update
  8.7 0.8 copy.39
  9.5 0.1 eq.31
  9.7 0.2 fusion
  9.9 0.1 convert_element_type.57
  10.0 0.1 copy.40
  10.1 0.7 multiply_add_fusion
  10.8 0.8 select_reduce_fusion
  11.6 0.1 copy.41
  11.8 0.2 copy.42
  12.0 1.9 negate_select_fusion
  13.9 0.0 copy-done.3
  13.9 0.0 copy-done.4
  13.9 0.0 copy-start.2
  13.9 0.0 copy-start.5
  13.9 1.1 fusion.7
  15.0 25.9 %shard_map.190 = bf16[128,1024]{1,0:T(8,128)(2,1)} custom-call(bf16[512,128]{1,0:T(8,128)(2,1)} %q_ref.1, bf16[512,128]{1,0:T(8,128)(2,1)} %k_ref.1, bf16[512,256]{1,0:T(8,128)(2,1)} %v_ref.1, bf16[512,256]{1,0:T(8,128)(2,1)} %gate_ref.2, f32[512,128]{1,0:T(8,128)} %get-tuple-element.17.fwd_ref, f32[512,128]{1,0:T(8,128)} %get-tuple-element.18.bwd_ref, ...), custom_call_target="tpu_custom_call" | custom-call | tf_op jit(solution)/shard_map/pallas_call | solution.py:259
  40.9 0.0 copy-start.6
  40.9 0.1 fusion.5
  41.1 3.1 %multiply_reduce_fusion = (f32[128]{0:T(128)S(1)}, f32[128,2048]{1,0:T(8,128)S(1)}) fusion(bf16[128,1024]{1,0:T(8,128)(2,1)} %shard_map.190, bf16[1024,2048]{1,0:T(8,128)(2,1)} %param.28), kind=kOutput, calls=%fused_computation.9 | convolution fusion | flops 537395072 | bytes 5505536 | tf_op jit(solution)/shard_map/dot_general | solution.py:600
  44.2 0.0 copy-done.2
  44.2 0.0 copy-done.5
  44.2 0.4 fusion.1
  44.6 0.0 copy-start.1
  44.6 0.0 copy-done.6
  44.6 0.2 fusion.3.rows_ref
  44.8 0.0 copy-start
  44.8 1.8 convolution_convert_fusion
  46.6 0.0 copy-done
  46.6 82.1 %shard_map.191 = (bf16[8,48,2048]{2,1,0:T(8,128)(2,1)}, f32[128,2048]{1,0:T(8,128)}) custom-call(bf16[8,48,2048]{2,1,0:T(8,128)(2,1)} %bitcast.16, bf16[128,2048]{1,0:T(8,128)(2,1)} %copy-done, bf16[2048,128]{1,0:T(8,128)(2,1)} %gate_ref.3, bf16[2048,128]{1,0:T(8,128)(2,1)} %up_ref.1, bf16[128,2048]{1,0:T(8,128)(2,1)} %down_ref.1), custom_call_target="tpu_custom_call" | custom-call | tf_op jit(solution)/shard_map/pallas_call | solution.py:379
  128.7 0.9 fusion.4
  129.6 0.0 all-gather.5.cloned.1.call-done.gate_hbm
  129.6 0.0 all-gather.7.cloned.1.call-done.up_hbm
  129.6 15.8 %all-gather.9.cloned.1.call-done = bf16[1,1024,2048]{2,1,0:T(8,128)(2,1)} async-done(((bf16[1,256,2048]{2,1,0:T(8,128)(2,1)}), bf16[1,1024,2048]{2,1,0:T(8,128)(2,1)}) %all-gather.9.cloned.1.call-update) | async-done | bytes 4194320 | tf_op jit(solution)/shard_map/all_gather | solution.py:572
  145.4 0.0 copy-done.1
  145.4 49.3 %shard_map.192 = bf16[128,2048]{1,0:T(8,128)(2,1)} custom-call(bf16[384,2048]{1,0:T(8,128)(2,1)} %bitcast.18, bf16[4,2048,256]{2,1,0:T(8,128)(2,1)} %all-gather.5.cloned.1.call-done.gate_hbm, bf16[4,2048,256]{2,1,0:T(8,128)(2,1)} %all-gather.7.cloned.1.call-done.up_hbm, bf16[1024,2048]{1,0:T(8,128)(2,1)} %bitcast.17, ...), custom_call_target="tpu_custom_call" | custom-call | tf_op jit(solution)/shard_map/pallas_call | solution.py:511
  194.7 1.9 copy.44
  (6 shorter events, 0.0 us)
Async XLA Ops:
  6.5 7.3 %copy-start.3 = (f32[512,128]{1,0:T(8,128)S(1)}, f32[512,128]{1,0:T(8,128)}, u32[]{:S(2)}) copy-start(f32[512,128]{1,0:T(8,128)} %param.25) | copy-start | bytes 786436
  6.5 7.3 %copy-start.4 = (f32[512,128]{1,0:T(8,128)S(1)}, f32[512,128]{1,0:T(8,128)}, u32[]{:S(2)}) copy-start(f32[512,128]{1,0:T(8,128)} %param.26) | copy-start | bytes 786436
  6.5 123.1 %all-gather.5.cloned.1.call-start = ((), (), s32[]{:S(2)}) async-start(), calls=%async_computation | async-start | bytes 5242880 | tf_op jit(solution)/shard_map/all_gather | solution.py:570
  7.3 122.4 %all-gather.7.cloned.1.call-start = ((), (), s32[]{:S(2)}) async-start(), calls=%async_computation.1 | async-start | bytes 5242880 | tf_op jit(solution)/shard_map/all_gather | solution.py:571
  8.0 137.4 %all-gather.9.cloned.1.call-start = ((), (), s32[]{:S(2)}) async-start(), calls=%async_computation.2 | async-start | bytes 5242880 | tf_op jit(solution)/shard_map/all_gather | solution.py:572
  13.9 30.3 %copy-start.2 = (bf16[128,2048]{1,0:T(8,128)(2,1)S(1)}, bf16[128,2048]{1,0:T(8,128)(2,1)}, u32[]{:S(2)}) copy-start(bf16[128,2048]{1,0:T(8,128)(2,1)} %param.20) | copy-start | bytes 1572868
  13.9 30.3 %copy-start.5 = (f32[2048]{0:T(1024)S(1)}, f32[2048]{0:T(1024)}, u32[]{:S(2)}) copy-start(f32[2048]{0:T(1024)} %param.29) | copy-start | bytes 24580
  40.9 3.6 %copy-start.6 = (f32[2048]{0:T(1024)S(1)}, f32[2048]{0:T(1024)}, u32[]{:S(2)}) copy-start(f32[2048]{0:T(1024)} %param.30) | copy-start | bytes 24580
  44.6 100.9 %copy-start.1 = (bf16[128,2048]{1,0:T(8,128)(2,1)}, bf16[128,2048]{1,0:T(8,128)(2,1)S(1)}, u32[]{:S(2)}) copy-start(bf16[128,2048]{1,0:T(8,128)(2,1)S(1)} %get-tuple-element.12.residual_ref) | copy-start | bytes 1572868
  44.8 1.8 copy-start
Sparse Core Ops, SparseCore 0:
  8.9 38.3 all-gather.4
  48.9 55.7 all-gather.6
  106.2 39.1 all-gather.8

commit v4 on v3

--- a/solution.py
+++ b/solution.py
@@ -289,16 +289,13 @@
     down_ref,
     arrived_ref,
     shared_ref,
+    part_ref,
     block_land,
     row_land,
-    part_ref,
-    part_land,
     block_send,
     block_recv,
     row_send,
     row_recv,
-    part_send,
-    part_recv,
 ):
     sp_me = lax.axis_index("sp")
     tp_me = lax.axis_index("tp")
@@ -316,7 +313,7 @@
         pl.semaphore_signal(barrier, inc=1, device_id=tp_peer(step), device_id_type=MESH)
     pl.semaphore_wait(barrier, sp_count - 1 + tp_count - 1)
 
-    row_copies, block_copies, part_copies = [], [], []
+    row_copies, block_copies = [], []
     for step in range(1, tp_count):
         copy = pltpu.make_async_remote_copy(
             src_ref=rows_ref,
@@ -353,19 +350,7 @@
     for step in range(1, tp_count):
         row_copies[step - 1].wait()
         part_ref[step] = partial(row_land[step]).astype(jnp.bfloat16)
-        copy = pltpu.make_async_remote_copy(
-            src_ref=part_ref.at[step],
-            dst_ref=part_land.at[step],
-            send_sem=part_send.at[step],
-            recv_sem=part_recv.at[step],
-            device_id=tp_peer(tp_count - step),
-            device_id_type=MESH,
-        )
-        copy.start()
-        part_copies.append(copy)
-    for step in range(1, tp_count):
-        part_copies[step - 1].wait()
-        shared_ref[...] += part_land[step].astype(jnp.float32)
+    part_ref[0] = jnp.zeros(part_ref.shape[1:], part_ref.dtype)
     for copy in block_copies:
         copy.wait()
     arrived_ref[...] = block_land[...]
@@ -381,20 +366,17 @@
         out_shape=(
             jax.ShapeDtypeStruct(outgoing.shape, outgoing.dtype),
             jax.ShapeDtypeStruct(normed.shape, jnp.float32),
+            jax.ShapeDtypeStruct((tp_count,) + normed.shape, normed.dtype),
         ),
         in_specs=[vmem] * 5,
-        out_specs=(vmem, vmem),
+        out_specs=(vmem, vmem, vmem),
         scratch_shapes=[
             pltpu.VMEM(outgoing.shape, outgoing.dtype),
-            several,
-            several,
             several,
             pltpu.SemaphoreType.DMA((sp_count,)),
             pltpu.SemaphoreType.DMA((sp_count,)),
             pltpu.SemaphoreType.DMA((tp_count,)),
             pltpu.SemaphoreType.DMA((tp_count,)),
-            pltpu.SemaphoreType.DMA((tp_count,)),
-            pltpu.SemaphoreType.DMA((tp_count,)),
         ],
         compiler_params=pltpu.CompilerParams(collective_id=1, has_side_effects=True),
     )(outgoing, normed, shared_gate, shared_up, shared_down)
@@ -402,6 +384,7 @@
 
 def expert_kernel(
     sp_count,
+    tp_count,
     rows_ref,
     gate_hbm,
     up_hbm,
@@ -409,6 +392,7 @@
     high_ref,
     low_ref,
     shared_ref,
+    part_ref,
     residual_ref,
     gain_ref,
     out_ref,
@@ -418,9 +402,12 @@
     total_ref,
     done_ref,
     back_ref,
+    part_land,
     weight_sem,
     send_sem,
     recv_sem,
+    part_send,
+    part_recv,
 ):
     sp_me = lax.axis_index("sp")
     tp_me = lax.axis_index("tp")
@@ -447,6 +434,27 @@
             device_id=(lax.rem(sp_me + step, sp_count), tp_me),
             device_id_type=MESH,
         )
+
+    for step in range(1, tp_count):
+        pl.semaphore_signal(
+            barrier,
+            inc=1,
+            device_id=(sp_me, lax.rem(tp_me + step, tp_count)),
+            device_id_type=MESH,
+        )
+    pl.semaphore_wait(barrier, sp_count - 1 + tp_count - 1)
+    part_copies = []
+    for step in range(1, tp_count):
+        copy = pltpu.make_async_remote_copy(
+            src_ref=part_ref.at[step],
+            dst_ref=part_land.at[step],
+            send_sem=part_send.at[step],
+            recv_sem=part_recv.at[step],
+            device_id=(sp_me, lax.rem(tp_me + tp_count - step, tp_count)),
+            device_id_type=MESH,
+        )
+        copy.start()
+        part_copies.append(copy)
 
     for group in range(groups):
         for copy in fetches[group]:
@@ -469,7 +477,6 @@
             done_ref.dtype
         )
 
-    pl.semaphore_wait(barrier, sp_count - 1)
     copies = []
     for step in range(1, sp_count):
         target = lax.rem(sp_me + step, sp_count)
@@ -488,6 +495,9 @@
         copy.wait()
 
     mixture = shared_ref[...]
+    for step in range(1, tp_count):
+        part_copies[step - 1].wait()
+        mixture = mixture + part_land[step].astype(jnp.float32)
     for expert in range(sp_count):
         mixture = mixture + jnp.dot(
             high_ref[expert], back_ref[expert], preferred_element_type=jnp.float32
@@ -502,16 +512,16 @@
     ).astype(out_ref.dtype)
 
 
-def run_expert(rows, gate_parts, up_parts, down_mat, high, low, shared_sum, residual, gain):
+def run_expert(rows, gate_parts, up_parts, down_mat, high, low, shared_sum, parts, residual, gain):
     sp_count = lax.axis_size("sp")
     groups = gate_parts.shape[0]
     vmem = pl.BlockSpec(memory_space=pltpu.VMEM)
     hbm = pl.BlockSpec(memory_space=pl.ANY)
     blocked = pltpu.VMEM((sp_count, rows.shape[0] // sp_count, rows.shape[1]), rows.dtype)
     return pl.pallas_call(
-        functools.partial(expert_kernel, sp_count),
+        functools.partial(expert_kernel, sp_count, lax.axis_size("tp")),
         out_shape=jax.ShapeDtypeStruct(residual.shape, residual.dtype),
-        in_specs=[vmem, hbm, hbm, hbm] + [vmem] * 5,
+        in_specs=[vmem, hbm, hbm, hbm] + [vmem] * 6,
         out_specs=vmem,
         scratch_shapes=[
             pltpu.VMEM(gate_parts.shape, gate_parts.dtype),
@@ -520,12 +530,15 @@
             pltpu.VMEM(rows.shape, jnp.float32),
             blocked,
             blocked,
+            pltpu.VMEM(parts.shape, parts.dtype),
             pltpu.SemaphoreType.DMA((3, groups)),
             pltpu.SemaphoreType.DMA((sp_count,)),
             pltpu.SemaphoreType.DMA((sp_count,)),
+            pltpu.SemaphoreType.DMA((parts.shape[0],)),
+            pltpu.SemaphoreType.DMA((parts.shape[0],)),
         ],
         compiler_params=pltpu.CompilerParams(collective_id=2, has_side_effects=True),
-    )(rows, gate_parts, up_parts, down_mat, high, low, shared_sum, residual, gain)
+    )(rows, gate_parts, up_parts, down_mat, high, low, shared_sum, parts, residual, gain)
 
 
 def slot_map(route_block, experts, capacity):
@@ -604,7 +617,7 @@
     outgoing = lax.dot_general(
         pick, normed, (((0,), (0,)), ((), ())), preferred_element_type=jnp.float32
     ).astype(jnp.bfloat16)
-    arrived, shared_sum = dispatch(
+    arrived, shared_sum, parts = dispatch(
         outgoing.reshape(experts, capacity, model_width),
         normed,
         shared_gate,
@@ -619,6 +632,7 @@
         weights_high,
         weights_low,
         shared_sum,
+        parts,
         residual,
         moe_gain.reshape(1, -1),
     )

time: 203 us -> 196 us (0.966)
  Pallas kernels: 157 us -> 123 us
  waiting for transfers between devices: 17.9 us -> 44.9 us
    pallas_call x1, Pallas kernels: 82.1 us -> 45.7 us  [dispatch(): pl.pallas_call(functools.partial(dispatch_kernel, sp_count, tp_count), ou...]
    all_gather x1, waiting for transfers between devices: 15.8 us -> 35.4 us  [body(): down_mat = lax.all_gather(expert_down[0], 'tp', axis=0, tiled=True)]
    all_gather x1, waiting for transfers between devices: 0.01 us -> 7.34 us  [body(): up_parts = lax.all_gather(expert_up[0], 'tp')]
  transfers between devices with their start and end apart: 3 -> 3, of which waited for: 1 -> 2; matrix products, arithmetic and copies ran while one was open for 6% -> 6% of each run, Pallas kernels for 53% -> 37%
where the time goes in v4:
time: 196 us; the launch traced here: 195 us
  Pallas kernels  123 us (63%)
  waiting for transfers between devices  44.9 us (23%)
  between operations  13.3 us (7%)
  other arithmetic  6.11 us (3%)
  matrix products  5.04 us (3%)
  local copies, waits for them, and re-layouts  3.35 us (2%)
    pallas_call x1, Pallas kernels, run_expert(): pl.pallas_call(functools.partial(expert_kernel, sp_count, lax.axis_size('...  51 us
    pallas_call x1, Pallas kernels, dispatch(): pl.pallas_call(functools.partial(dispatch_kernel, sp_count, tp_count), ou...  45.7 us
    all_gather x1, waiting for transfers between devices, body(): down_mat = lax.all_gather(expert_down[0], 'tp', axis=0, tiled=True)  35.4 us
    pallas_call x1, Pallas kernels, attention(): pl.pallas_call(functools.partial(attention_kernel, sp_count, tp_count), o...  25.9 us
    all_gather x1, waiting for transfers between devices, body(): up_parts = lax.all_gather(expert_up[0], 'tp')  7.34 us
  transfers between devices with their start and end apart: 3, of which 2 were waited for; matrix products, arithmetic and copies ran while one was open for 6% of the time, Pallas kernels for 37%

profile of v4, /device:TPU:10, one launch (start us, length us, event | category | flops | bytes accessed | tf_op | source)
XLA Modules:
  0.0 195.3 jit_solution(17968594633149369453)
XLA Ops:
  6.5 0.0 copy-start.3
  6.5 0.0 copy-start.4
  6.5 0.0 all-gather.5.cloned.1.call-start
  6.5 0.7 all-gather.5.cloned.1.call-update
  7.3 0.0 all-gather.7.cloned.1.call-start
  7.3 0.7 all-gather.7.cloned.1.call-update
  8.0 0.0 all-gather.9.cloned.1.call-start
  8.1 0.7 all-gather.9.cloned.1.call-update
  8.7 0.8 copy.39
  9.5 0.1 eq.31
  9.7 0.2 fusion
  9.9 0.1 convert_element_type.57
  10.0 0.1 copy.40
  10.1 0.7 multiply_add_fusion
  10.8 0.8 select_reduce_fusion
  11.6 0.1 copy.41
  11.8 0.2 copy.42
  12.0 1.9 negate_select_fusion
  13.9 0.0 copy-done.3
  13.9 0.0 copy-done.4
  13.9 0.0 copy-start.2
  13.9 0.0 copy-start.5
  13.9 1.1 fusion.7
  15.0 25.9 %shard_map.190 = bf16[128,1024]{1,0:T(8,128)(2,1)} custom-call(bf16[512,128]{1,0:T(8,128)(2,1)} %q_ref.1, bf16[512,128]{1,0:T(8,128)(2,1)} %k_ref.1, bf16[512,256]{1,0:T(8,128)(2,1)} %v_ref.1, bf16[512,256]{1,0:T(8,128)(2,1)} %gate_ref.2, f32[512,128]{1,0:T(8,128)} %get-tuple-element.19.fwd_ref, f32[512,128]{1,0:T(8,128)} %get-tuple-element.20.bwd_ref, ...), custom_call_target="tpu_custom_call" | custom-call | tf_op jit(solution)/shard_map/pallas_call | solution.py:259
  40.9 0.0 copy-start.6
  40.9 0.1 fusion.5
  41.1 3.1 %multiply_reduce_fusion = (f32[128]{0:T(128)S(1)}, f32[128,2048]{1,0:T(8,128)S(1)}) fusion(bf16[128,1024]{1,0:T(8,128)(2,1)} %shard_map.190, bf16[1024,2048]{1,0:T(8,128)(2,1)} %param.28), kind=kOutput, calls=%fused_computation.9 | convolution fusion | flops 537395072 | bytes 5505536 | tf_op jit(solution)/shard_map/dot_general | solution.py:613
  44.2 0.0 copy-done.2
  44.2 0.0 copy-done.5
  44.2 0.4 fusion.1
  44.6 0.0 copy-start
  44.6 0.0 copy-done.6
  44.6 0.2 fusion.3.rows_ref
  44.8 0.0 copy-start.1
  44.8 1.8 convolution_convert_fusion
  46.5 0.0 copy-done.1
  46.5 45.7 %shard_map.191 = (bf16[8,48,2048]{2,1,0:T(8,128)(2,1)}, f32[128,2048]{1,0:T(8,128)}, bf16[4,128,2048]{2,1,0:T(8,128)(2,1)}) custom-call(bf16[8,48,2048]{2,1,0:T(8,128)(2,1)} %bitcast.16, bf16[128,2048]{1,0:T(8,128)(2,1)} %copy-done.1, bf16[2048,128]{1,0:T(8,128)(2,1)} %gate_ref.3, bf16[2048,128]{1,0:T(8,128)(2,1)} %up_ref.1, bf16[128,2048]{1,0:T(8,128)(2,1)} %down_ref.1), custom_call_target="tpu_custom_call" | custom-call | tf_op jit(solution)/shard_map/pallas_call | solution.py:364
  92.2 0.9 fusion.4
  93.1 0.0 all-gather.5.cloned.1.call-done.gate_hbm
  93.1 7.3 %all-gather.7.cloned.1.call-done.up_hbm = bf16[4,2048,256]{2,1,0:T(8,128)(2,1)} async-done(((bf16[1,2048,256]{2,1,0:T(8,128)(2,1)}), bf16[4,2048,256]{2,1,0:T(8,128)(2,1)}) %all-gather.7.cloned.1.call-update) | async-done | bytes 4194320 | tf_op jit(solution)/shard_map/all_gather | solution.py:584
  100.5 35.4 %all-gather.9.cloned.1.call-done = bf16[1,1024,2048]{2,1,0:T(8,128)(2,1)} async-done(((bf16[1,256,2048]{2,1,0:T(8,128)(2,1)}), bf16[1,1024,2048]{2,1,0:T(8,128)(2,1)}) %all-gather.9.cloned.1.call-update) | async-done | bytes 4194320 | tf_op jit(solution)/shard_map/all_gather | solution.py:585
  135.9 0.0 copy-done
  135.9 51.0 %shard_map.192 = bf16[128,2048]{1,0:T(8,128)(2,1)} custom-call(bf16[384,2048]{1,0:T(8,128)(2,1)} %bitcast.18, bf16[4,2048,256]{2,1,0:T(8,128)(2,1)} %all-gather.5.cloned.1.call-done.gate_hbm, bf16[4,2048,256]{2,1,0:T(8,128)(2,1)} %all-gather.7.cloned.1.call-done.up_hbm, bf16[1024,2048]{1,0:T(8,128)(2,1)} %bitcast.17, ...), custom_call_target="tpu_custom_call" | custom-call | tf_op jit(solution)/shard_map/pallas_call | solution.py:521
  186.9 1.9 copy.44
  (6 shorter events, 0.0 us)
Async XLA Ops:
  6.5 7.3 %copy-start.3 = (f32[512,128]{1,0:T(8,128)S(1)}, f32[512,128]{1,0:T(8,128)}, u32[]{:S(2)}) copy-start(f32[512,128]{1,0:T(8,128)} %param.25) | copy-start | bytes 786436
  6.5 7.3 %copy-start.4 = (f32[512,128]{1,0:T(8,128)S(1)}, f32[512,128]{1,0:T(8,128)}, u32[]{:S(2)}) copy-start(f32[512,128]{1,0:T(8,128)} %param.26) | copy-start | bytes 786436
  6.5 86.6 %all-gather.5.cloned.1.call-start = ((), (), s32[]{:S(2)}) async-start(), calls=%async_computation | async-start | bytes 5242880 | tf_op jit(solution)/shard_map/all_gather | solution.py:583
  7.3 93.2 %all-gather.7.cloned.1.call-start = ((), (), s32[]{:S(2)}) async-start(), calls=%async_computation.1 | async-start | bytes 5242880 | tf_op jit(solution)/shard_map/all_gather | solution.py:584
  8.0 127.9 %all-gather.9.cloned.1.call-start = ((), (), s32[]{:S(2)}) async-start(), calls=%async_computation.2 | async-start | bytes 5242880 | tf_op jit(solution)/shard_map/all_gather | solution.py:585
  13.9 30.3 %copy-start.2 = (bf16[128,2048]{1,0:T(8,128)(2,1)S(1)}, bf16[128,2048]{1,0:T(8,128)(2,1)}, u32[]{:S(2)}) copy-start(bf16[128,2048]{1,0:T(8,128)(2,1)} %param.20) | copy-start | bytes 1572868
  13.9 30.3 %copy-start.5 = (f32[2048]{0:T(1024)S(1)}, f32[2048]{0:T(1024)}, u32[]{:S(2)}) copy-start(f32[2048]{0:T(1024)} %param.29) | copy-start | bytes 24580
  40.9 3.6 %copy-start.6 = (f32[2048]{0:T(1024)S(1)}, f32[2048]{0:T(1024)}, u32[]{:S(2)}) copy-start(f32[2048]{0:T(1024)} %param.30) | copy-start | bytes 24580
  44.6 91.3 %copy-start = (bf16[128,2048]{1,0:T(8,128)(2,1)}, bf16[128,2048]{1,0:T(8,128)(2,1)S(1)}, u32[]{:S(2)}) copy-start(bf16[128,2048]{1,0:T(8,128)(2,1)S(1)} %get-tuple-element.14.residual_ref) | copy-start | bytes 1572868
  44.8 1.8 copy-start.1
Sparse Core Ops, SparseCore 0:
  8.9 38.3 all-gather.4
  48.9 51.5 all-gather.6
  102.0 33.8 all-gather.8
